TPU v7x, 32 devices: a whole 2x2x4 slice. The times are simulated.
32 devices in a mesh: grp: 2 (over y), fs: 4 (over z), tp: 4 (over x, core).
Axes of the slice: x: 2, y: 2, z: 4, core: 2. Of those that a mesh axis runs over, the one named last changes fastest.
Arguments:
- tokens: bfloat16 [2048, 3072], P(('grp', 'tp')), parts along dimension 0, may hold values from -6 to 6
- up_master: float32 [3072, 12288], P('fs', 'tp'), may hold values from -0.109375 to 0.109375
- down_master: float32 [12288, 3072], P('fs', 'tp'), may hold values from -0.0546875 to 0.0546875
- norm_gain: float32 [3072], P('fs'), may hold values from 0.1 to 1.9
Outputs:
- prompt_out: bfloat16 [2048, 3072], P(('grp', 'tp'), 'fs'), parts along dimension 0
- sampled_up: bfloat16 [6144, 12288], P('grp', 'fs'), parts along dimension 0
- sampled_down: bfloat16 [24576, 3072], P(('grp', 'fs')), parts along dimension 0
There are 2 independent parts, one for each index of `grp`. A program takes and returns all parts, laid end to end along the dimension named above; an argument that names none is the same for every part. Nothing has to cross between parts.
All inputs are finite; a program needn't handle non-finite values.
Results may differ from a plain program's by a relative error of at most 0.0074.
Values may be sent and summed in bfloat16 or wider, within the bound.
A program may use at most 192 MiB of HBM per device.

v0:
```python
import functools

import jax
import jax.numpy as jnp
from jax import lax
from jax.experimental import pallas as pl
from jax.experimental.pallas import tpu as pltpu
from jax.sharding import PartitionSpec as P

MESH = pl.DeviceIdType.MESH
CORES = 2
LAG = 2
EARLY = 2
UNIT = 256
LIMIT = 22


def normalize(tokens):
    values = tokens.astype(jnp.float32)
    center = jnp.mean(values, axis=-1, keepdims=True)
    spread = jnp.mean(jnp.square(values - center), axis=-1, keepdims=True)
    return ((values - center) * lax.rsqrt(spread + 1e-05)).astype(jnp.bfloat16)


def pieces_of(size, unit, most):
    for count in range(most, 1, -1):
        if size % (count * unit) == 0:
            return count
    return 1


def hand_over(dims, cuts, tokens_ref, up_ref, master_ref, got_up, got_down, out_ref, rows_ref, taken, down_ref, hidden, mine, sent, landed, up_sems, down_sems, sum_sems, local_sem, take_sem):
    groups, fs, tp = dims
    pairs = tp // CORES
    up_cuts, down_cuts = cuts
    y, f, t = lax.axis_index("grp"), lax.axis_index("fs"), lax.axis_index("tp")
    x, k = t // CORES, t % CORES
    first_send, first_recv, x_send, y_send, y_recv, a_send, a_recv, b_send, b_recv = up_sems
    own_send, own_recv, dx_send, dx_recv, dy_send, dy_recv, da_send, da_recv, db_send, db_recv = down_sems
    sum_send, sum_recv = sum_sems
    cols = up_ref.shape[2] // up_cuts
    depth = got_up.shape[0] * got_up.shape[1] * got_up.shape[2]
    home = f // CORES
    sibling = (y, f, x * CORES + (1 - k))

    def remote(src, dst, send, recv, where):
        return pltpu.make_async_remote_copy(src_ref=src, dst_ref=dst, send_sem=send, recv_sem=recv, device_id=where, device_id_type=MESH)

    height = down_ref.shape[0] // groups
    width = down_ref.shape[1]
    tile = width // down_cuts

    def down_at(ref, group, cut, column):
        return ref.at[pl.ds(pl.multiple_of(group * height, height), height), pl.ds(pl.multiple_of(column * width + cut * tile, tile), tile)]

    def from_pair(dx):
        return ((x - dx + pairs) % pairs) * CORES + k

    def down_first(dx, cut):
        return remote(down_at(down_ref, y, cut, 0), down_at(got_down, y, cut, t), dx_send.at[dx - 1, cut], dx_recv.at[dx - 1, cut], (y, f, ((x + dx) % pairs) * CORES + k))

    def down_y(dx, dy, cut):
        here = down_at(got_down, y, cut, from_pair(dx))
        return remote(here, here, dy_send.at[dx - 1, dy - 1, cut], dy_recv.at[dx - 1, dy - 1, cut], ((y + dy) % groups, f, t))

    def down_a(dx, cut):
        here = down_at(got_down, y, cut, from_pair(dx))
        return remote(here, here, da_send.at[dx - 1, cut], da_recv.at[dx - 1, cut], sibling)

    def down_b(dx, dy, cut):
        here = down_at(got_down, (y - dy + groups) % groups, cut, from_pair(dx))
        return remote(here, here, db_send.at[dx - 1, dy - 1, cut], db_recv.at[dx - 1, dy - 1, cut], sibling)

    own_columns = got_down.at[:, pl.ds(pl.multiple_of(t * width, width), width)]
    down_own = remote(down_ref, own_columns, own_send, own_recv, sibling)
    down_here = pltpu.make_async_copy(down_ref, own_columns, local_sem)

    def up_at(ref, group, lane, cut):
        return ref.at[group * CORES + lane, :, pl.ds(cut * cols, cols)]

    def up_first(lane, cut):
        return remote(up_at(up_ref, y, lane, cut), up_at(got_up.at[f], y, lane, cut), first_send.at[lane, cut], first_recv.at[f, cut], (y, t, x * CORES + lane))

    def up_here(r, cut):
        return pltpu.make_async_copy(up_at(up_ref, y, k, cut), up_at(got_up.at[r], y, k, cut), first_recv.at[r, cut])

    def up_x(r, cut, dx):
        here = up_at(got_up.at[r], y, k, cut)
        return remote(here, here, x_send.at[dx - 1, r, cut], first_recv.at[r, cut], (y, f, ((x + dx) % pairs) * CORES + k))

    def up_y(r, cut, dy):
        here = up_at(got_up.at[r], y, k, cut)
        return remote(here, here, y_send.at[dy - 1, r, cut], y_recv.at[dy - 1, r, cut], ((y + dy) % groups, f, t))

    def up_a(r, cut):
        here = up_at(got_up.at[r], y, k, cut)
        return remote(here, here, a_send.at[r, cut], a_recv.at[r, cut], sibling)

    def up_b(r, cut, dy):
        here = up_at(got_up.at[r], (y - dy + groups) % groups, k, cut)
        return remote(here, here, b_send.at[dy - 1, r, cut], b_recv.at[dy - 1, r, cut], sibling)

    def is_self(lane):
        return jnp.logical_and(t == f, lane == k)

    def hidden_units(cut):
        @pl.loop(0, cols // UNIT)
        def _(step):
            at = pl.ds(pl.multiple_of(cut * cols + step * UNIT, UNIT), UNIT)
            block = got_up[:, :, :, at].reshape(depth, UNIT)
            before = jnp.dot(rows_ref[...], block, preferred_element_type=jnp.float32)
            hidden[:, at] = jnp.square(jnp.maximum(before, 0.0)).astype(jnp.bfloat16)

    def sum_to(column, cut):
        at = pl.ds(cut * tile, tile)
        return remote(sent.at[column, :, at], landed.at[f, :, at], sum_send.at[column, cut], sum_recv.at[f, cut], (y, column, t))

    def features(column, cut):
        at = pl.ds(pl.multiple_of(column * width + cut * tile, tile), tile)
        term = jnp.dot(hidden[...], got_down[:, at], preferred_element_type=jnp.float32)

        @pl.when(column == f)
        def _():
            mine[:, pl.ds(cut * tile, tile)] = term

        @pl.when(column != f)
        def _():
            sent[column, :, pl.ds(cut * tile, tile)] = term.astype(jnp.bfloat16)
            sum_to(column, cut).start()

    early = min(EARLY, down_cuts)
    for lane in range(CORES):
        @pl.when(is_self(lane))
        def _():
            for cut in range(up_cuts):
                up_here(f, cut).start()
    for cut in range(up_cuts):
        for lane in range(CORES):
            @pl.when(jnp.logical_not(is_self(lane)))
            def _():
                up_first(lane, cut).start()

    slab = taken.shape[1]
    slabs = down_ref.shape[0] // slab

    def take(step, slot):
        return pltpu.make_async_copy(master_ref.at[pl.ds(step * slab, slab), :], taken.at[slot], take_sem.at[slot])

    take(0, 0).start()
    for step in range(slabs):
        slot = step % 2
        if step + 1 < slabs:
            take(step + 1, 1 - slot).start()
        take(step, slot).wait()

        @pl.loop(0, slab // 16)
        def _(line):
            start = pl.multiple_of(line * 16, 16)
            down_ref[pl.ds(pl.multiple_of(step * slab + start, 16), 16), :] = taken[slot, pl.ds(start, 16), :].astype(jnp.bfloat16)

    for cut in range(early):
        for dx in range(1, pairs):
            down_first(dx, cut).start()
    down_here.start()
    down_own.start()

    @pl.when(x != home)
    def _():
        for cut in range(early, down_cuts):
            for dx in range(1, pairs):
                down_first(dx, cut).start()

    @pl.loop(0, tokens_ref.shape[0] // 16)
    def _(step):
        at = pl.ds(pl.multiple_of(step * 16, 16), 16)
        rows_ref[at, :] = normalize(tokens_ref[at, :])

    order = [(0, cut) for cut in range(up_cuts)] + [(j, cut) for cut in range(up_cuts) for j in range(1, fs)]

    def up_arrival(j, cut):
        r = (f + j) % fs
        up_here(r, cut).wait()

        @pl.when(x == home)
        def _():
            for dx in range(1, pairs):
                up_x(r, cut, dx).start()

        for dy in range(1, groups):
            up_y(r, cut, dy).start()
        up_a(r, cut).start()

    def up_second(j, cut):
        r = (f + j) % fs
        for dy in range(1, groups):
            up_y(r, cut, dy).wait_recv()
            up_b(r, cut, dy).start()

    def up_done(cut):
        for j in range(fs):
            r = (f + j) % fs
            up_a(r, cut).wait_recv()
            for dy in range(1, groups):
                up_b(r, cut, dy).wait_recv()
        hidden_units(cut)

    done = 0
    for step in range(len(order) + LAG):
        if step < len(order):
            up_arrival(*order[step])
        if step == len(order) - 1:
            @pl.when(x == home)
            def _():
                for cut in range(early, down_cuts):
                    for dx in range(1, pairs):
                        down_first(dx, cut).start()
        if step >= LAG:
            up_second(*order[step - LAG])
        if done < up_cuts - 1 and step == up_cuts + (done + 2) * (fs - 1) - 1:
            up_done(done)
            done += 1

    down_here.wait()
    for step in range(down_cuts + 2):
        if step < down_cuts:
            for dx in range(1, pairs):
                down_first(dx, step).wait_recv()
                for dy in range(1, groups):
                    down_y(dx, dy, step).start()
                down_a(dx, step).start()
        if step == 0:
            for cut in range(done, up_cuts):
                up_done(cut)
        if 1 <= step <= down_cuts:
            for dx in range(1, pairs):
                for dy in range(1, groups):
                    down_y(dx, dy, step - 1).wait_recv()
                    down_b(dx, dy, step - 1).start()
        if step < down_cuts:
            features(t, step)
            if step == 0:
                down_own.wait_recv()
            features(x * CORES + (1 - k), step)
        if 1 <= step <= down_cuts:
            for dx in range(1, pairs):
                features(from_pair(dx), step - 1)
        if step >= 2:
            for dx in range(1, pairs):
                down_a(dx, step - 2).wait_recv()
                for dy in range(1, groups):
                    down_b(dx, dy, step - 2).wait_recv()
                features(((x - dx + pairs) % pairs) * CORES + (1 - k), step - 2)

    for cut in range(down_cuts):
        at = pl.ds(cut * tile, tile)
        for j in range(1, fs):
            r = (f + j) % fs
            remote(sent.at[r, :, at], landed.at[r, :, at], sum_send.at[r, cut], sum_recv.at[r, cut], (y, r, t)).wait_recv()
        total = mine[:, at]
        for j in range(1, fs):
            total += landed[(f + j) % fs, :, at].astype(jnp.float32)
        out_ref[:, at] = total.astype(jnp.bfloat16)

    for cut in range(up_cuts):
        for j in range(fs):
            r = (f + j) % fs
            up_a(r, cut).wait_send()
            for dy in range(1, groups):
                up_b(r, cut, dy).wait_send()
                up_y(r, cut, dy).wait_send()

            @pl.when(x == home)
            def _():
                for dx in range(1, pairs):
                    up_x(r, cut, dx).wait_send()

        for lane in range(CORES):
            @pl.when(jnp.logical_not(is_self(lane)))
            def _():
                up_first(lane, cut).wait_send()
    for cut in range(down_cuts):
        for dx in range(1, pairs):
            down_first(dx, cut).wait_send()
            down_a(dx, cut).wait_send()
            for dy in range(1, groups):
                down_y(dx, dy, cut).wait_send()
                down_b(dx, dy, cut).wait_send()
        for j in range(1, fs):
            sum_to((f + j) % fs, cut).wait_send()
    down_own.wait_send()


def fused(tokens_in, up_cast, down_master, dims):
    groups, fs, tp = dims
    rows, cols = up_cast.shape[0] // (groups * CORES), up_cast.shape[1]
    height, width = down_master.shape
    tokens = tokens_in.shape[0]
    up_cuts = pieces_of(cols, UNIT, 4)
    down_cuts = pieces_of(width, 128, 6)
    pairs = tp // CORES
    dma = pltpu.SemaphoreType.DMA
    far = groups - 1
    up_sems = [dma((CORES, up_cuts)), dma((fs, up_cuts)), dma((pairs - 1, fs, up_cuts)), dma((far, fs, up_cuts)), dma((far, fs, up_cuts))]
    up_sems += [dma((fs, up_cuts)), dma((fs, up_cuts)), dma((far, fs, up_cuts)), dma((far, fs, up_cuts))]
    one, two = (pairs - 1, down_cuts), (pairs - 1, far, down_cuts)
    down_sems = [dma, dma, dma(one), dma(one), dma(two), dma(two), dma(one), dma(one), dma(two), dma(two)]
    vmem = pl.BlockSpec(memory_space=pltpu.VMEM)
    hbm = pl.BlockSpec(memory_space=pl.ANY)
    got_up, got_down, out = pl.pallas_call(
        functools.partial(hand_over, dims, (up_cuts, down_cuts)),
        out_shape=(
            pltpu.VMEM((fs, groups * CORES, rows, cols), jnp.bfloat16),
            pltpu.VMEM((height, tp * width), jnp.bfloat16),
            jax.ShapeDtypeStruct((tokens, width), jnp.bfloat16),
        ),
        in_specs=[vmem, hbm, hbm],
        out_specs=(vmem, vmem, vmem),
        scratch_shapes=[
            pltpu.VMEM(tokens_in.shape, jnp.bfloat16),
            pltpu.VMEM((2, height // pieces_of(height, 16, 12), width), jnp.float32),
            pltpu.VMEM((height, width), jnp.bfloat16),
            pltpu.VMEM((tokens, cols), jnp.bfloat16),
            pltpu.VMEM((tokens, width), jnp.float32),
            pltpu.VMEM((fs, tokens, width), jnp.bfloat16),
            pltpu.VMEM((fs, tokens, width), jnp.bfloat16),
            up_sems,
            down_sems,
            [dma((fs, down_cuts)), dma((fs, down_cuts))],
            dma,
            dma((2,)),
        ],
        compiler_params=pltpu.CompilerParams(has_side_effects=True, vmem_limit_bytes=LIMIT << 20),
    )(tokens_in, up_cast.reshape(groups * CORES, rows, cols), down_master)
    return out, got_up.reshape(fs * groups * CORES * rows, cols), got_down


def fits(up_shape, down_shape, dims):
    groups, fs, tp = dims
    own = 2 * (up_shape[0] * up_shape[1] * fs + down_shape[0] * down_shape[1] * tp)
    aligned = up_shape[0] % (groups * CORES * 16) == 0 and up_shape[1] % UNIT == 0
    return fs == tp and groups > 1 and tp % CORES == 0 and tp > CORES and aligned and down_shape[0] % (groups * 16) == 0 and down_shape[1] % 128 == 0 and own <= 40 << 20


def by_collectives(normalized, up_cast, down_cast):
    quarter = lax.all_to_all(up_cast, "tp", split_axis=0, concat_axis=1, tiled=True)
    moved = lax.all_to_all(quarter, "fs", split_axis=1, concat_axis=0, tiled=True)
    part_rows = quarter.shape[0]
    stacked = moved.reshape(moved.shape[0] // part_rows, part_rows, moved.shape[1])
    joined = lax.all_gather(stacked, "tp", axis=1, tiled=True)
    sampled_down = lax.all_gather(down_cast, "tp", axis=1, tiled=True)
    sampled_up = joined.reshape(joined.shape[0] * joined.shape[1], joined.shape[2])
    before = jnp.dot(normalized, sampled_up, preferred_element_type=jnp.float32)
    hidden = jnp.square(jax.nn.relu(before)).astype(jnp.bfloat16)
    terms = jnp.dot(hidden, sampled_down, preferred_element_type=jnp.float32)
    summed = lax.psum_scatter(terms, "fs", scatter_dimension=1, tiled=True)
    return summed.astype(jnp.bfloat16), sampled_up, sampled_down


def shards(dims, tokens, up_master, down_master, norm_gain):
    up_cast = (norm_gain[:, None] * up_master).astype(jnp.bfloat16)
    if fits(up_master.shape, down_master.shape, dims):
        return fused(tokens, up_cast, down_master, dims)
    return by_collectives(normalize(tokens), up_cast, down_master.astype(jnp.bfloat16))


def solution(mesh):
    dims = tuple(mesh.shape[name] for name in ("grp", "fs", "tp"))
    return jax.shard_map(
        functools.partial(shards, dims),
        mesh=mesh,
        in_specs=(P(("grp", "tp"), None), P("fs", "tp"), P("fs", "tp"), P("fs")),
        out_specs=(P(("grp", "tp"), "fs"), P("grp", "fs"), P(("grp", "fs"), None)),
        check_vma=False,
    )
```

profile of v0, /device:TPU:3, one launch (start us, length us, event | category | flops | bytes accessed | tf_op | source)
XLA Modules:
  0.0 236.9 jit_solution(3985455116428412876)
XLA Ops:
  0.6 7.3 %multiply_convert_fusion = bf16[768,3072]{1,0:T(8,128)(2,1)} fusion(f32[768,3072]{1,0:T(8,128)} %param.5, f32[768]{0:T(1024)} %param.7), kind=kLoop, calls=%fused_computation | loop fusion | flops 4718592 | bytes 14158848 | tf_op jit(solution)/shard_map/convert_element_type | solution.py:360
  7.9 214.5 %shard_map.67 = (bf16[4,4,192,3072]{3,2,1,0:T(8,128)(2,1)S(1)}, bf16[3072,3072]{1,0:T(8,128)(2,1)S(1)}, bf16[256,768]{1,0:T(8,128)(2,1)}) custom-call(bf16[256,3072]{1,0:T(8,128)(2,1)} %tokens_ref.1, bf16[4,192,3072]{2,1,0:T(8,128)(2,1)} %bitcast.3, f32[3072,768]{1,0:T(8,128)} %master_ref.1), custom_call_target="tpu_custom_call" | custom-call | tf_op jit(solution)/shard_map/pallas_call | solution.py:309
  222.5 6.9 %copy.10 = bf16[3072,3072]{1,0:T(8,128)(2,1)} copy(bf16[3072,3072]{1,0:T(8,128)(2,1)S(1)} %bitcast.2) | data formatting | bytes 37748736
  229.3 0.0 copy-start
  229.3 6.8 %copy.11 = bf16[3072,3072]{1,0:T(8,128)(2,1)} copy(bf16[3072,3072]{1,0:T(8,128)(2,1)S(1)} %get-tuple-element.11) | data formatting | bytes 37748736
  236.2 0.0 copy-done
  236.2 0.7 copy.12
Async XLA Ops:
  229.3 6.9 %copy-start = (bf16[256,768]{1,0:T(8,128)(2,1)S(1)}, bf16[256,768]{1,0:T(8,128)(2,1)}, u32[]{:S(2)}) copy-start(bf16[256,768]{1,0:T(8,128)(2,1)} %get-tuple-element.15) | copy-start | bytes 1179652
where the time goes:
time: 237 us
  Pallas kernels  215 us (91%)
  local copies, waits for them, and re-layouts  14.5 us (6%)
  other arithmetic  7.3 us (3%)
    pallas_call x1, Pallas kernels, fused(): pl.pallas_call(functools.partial(hand_over, dims, (up_cuts, down_cuts)),...  215 us
    unnamed x5, local copies, waits for them, and re-layouts  14.5 us
    convert_element_type x1, other arithmetic, shards(): up_cast = (norm_gain[:, None] * up_master).astype(jnp.bfloat16)  7.3 us

commit v1 on v0

v1 whole, which is shorter than its diff:
```python
import functools

import jax
import jax.numpy as jnp
from jax import lax
from jax.experimental import pallas as pl
from jax.experimental.pallas import tpu as pltpu
from jax.sharding import PartitionSpec as P

MESH = pl.DeviceIdType.MESH
CORES = 2
PLANES = 2
LAG = 3
UNIT = 256
LINE = 16
LIMIT = 24
UP_CUTS = 6
DOWN_CUTS = 6
SHARED = 8
SHARES = 16


def normalize(tokens):
    values = tokens.astype(jnp.float32)
    center = jnp.mean(values, axis=-1, keepdims=True)
    spread = jnp.mean(jnp.square(values - center), axis=-1, keepdims=True)
    return ((values - center) * lax.rsqrt(spread + 1e-05)).astype(jnp.bfloat16)


def pieces_of(size, unit, most):
    for count in range(most, 1, -1):
        if size % (count * unit) == 0:
            return count
    return 1


def shared_rows(height):
    return height * SHARED // SHARES // (2 * LINE) * (2 * LINE)


def up_order(fs, cuts):
    events = []
    for cut in range(cuts):
        at = (cut + 1) / cuts
        events.append((at, 0, "relay", 0, cut))
        for j in range(fs):
            pace = (1.0, 1.25, 2.0, 2.0)[j]
            events.append((at * pace, 1 + j, "arrive", j, cut))
    events.append((0.55, 9, "split", 0, 0))
    events.append((0.85, 9, "shared", 0, 0))
    return [event[2:] for event in sorted(events)]


def hand_over(dims, cuts, tokens_ref, gain_ref, up_ref, master_ref, got_up, got_down, out_ref, rows_ref, gains, up_stage, up_src, relayed, stage, hidden, keep, send1, recv1, send2, recv2, up_sems, down_sems, sum_sems, load_sems):
    groups, fs, tp = dims
    up_cuts, down_cuts = cuts
    y, f, t = lax.axis_index("grp"), lax.axis_index("fs"), lax.axis_index("tp")
    x, k = t // CORES, t % CORES
    home_send, cross_send, first_recv, relay_send, relay_recv, y_send, y_recv, a_send, a_recv, b_send, b_recv = up_sems
    own_send, own_recv, split_send, split_recv, shared_send, shared_recv, dy_send, dy_recv, da_send, da_recv, ds_send, ds_recv, db_send, db_recv = down_sems
    send1_send, send1_recv, send2_send, send2_recv = sum_sems
    load_up, load_down, load_tokens = load_sems
    rows, cols = up_src.shape[1], up_src.shape[2] // up_cuts
    depth = got_up.shape[0] * got_up.shape[1] * got_up.shape[2]
    height, width = master_ref.shape
    tile = width // down_cuts
    both = shared_rows(height)
    part = (height - both) // groups
    near = f + 1 - 2 * (f % 2)
    rows_from = (f, near, (f + 2) % fs, (near + 2) % fs)
    sibling = (y, f, x * CORES + (1 - k))
    across_y = (1 - y, f, t)
    other = (1 - x) * CORES
    across_x = (y, f, other + k)

    def remote(src, dst, send, recv, where):
        return pltpu.make_async_remote_copy(src_ref=src, dst_ref=dst, send_sem=send, recv_sem=recv, device_id=where, device_id_type=MESH)

    def up_at(ref, group, lane, cut):
        return ref.at[group * CORES + lane, :, pl.ds(cut * cols, cols)]

    def src_at(lane, cut):
        return up_src.at[lane, :, pl.ds(cut * cols, cols)]

    def up_load(lane, cut):
        at = pl.ds(cut * cols, cols)
        return pltpu.make_async_copy(up_ref.at[y * CORES + lane, :, at], up_stage.at[lane, :, at], load_up.at[lane, cut])

    def up_local(cut):
        return pltpu.make_async_copy(src_at(k, cut), up_at(got_up.at[f], y, k, cut), first_recv.at[f, cut])

    def up_home(lane, cut):
        return remote(src_at(lane, cut), up_at(got_up.at[f], y, lane, cut), home_send.at[lane, cut], first_recv.at[f, cut], (y, t, x * CORES + lane))

    def up_cross_own(lane, cut):
        return remote(src_at(lane, cut), up_at(got_up.at[f], y, lane, cut), cross_send.at[lane, cut], first_recv.at[f, cut], (y, f, other + lane))

    def up_cross(lane, cut):
        return remote(src_at(lane, cut), relayed.at[k, :, pl.ds(cut * cols, cols)], cross_send.at[lane, cut], relay_recv.at[k, cut], (y, f, other + lane))

    def up_relay(slot, cut):
        return remote(relayed.at[slot, :, pl.ds(cut * cols, cols)], up_at(got_up.at[f], y, k, cut), relay_send.at[slot, cut], first_recv.at[f, cut], (y, other + slot, t))

    def up_here(r, cut):
        return pltpu.make_async_copy(src_at(0, cut), up_at(got_up.at[r], y, k, cut), first_recv.at[r, cut])

    def relay_here(slot, cut):
        return pltpu.make_async_copy(src_at(0, cut), relayed.at[slot, :, pl.ds(cut * cols, cols)], relay_recv.at[slot, cut])

    def up_y(r, cut):
        here = up_at(got_up.at[r], y, k, cut)
        return remote(here, here, y_send.at[r, cut], y_recv.at[r, cut], across_y)

    def up_a(r, cut):
        here = up_at(got_up.at[r], y, k, cut)
        return remote(here, here, a_send.at[r, cut], a_recv.at[r, cut], sibling)

    def up_b(r, cut):
        here = up_at(got_up.at[r], 1 - y, k, cut)
        return remote(here, here, b_send.at[r, cut], b_recv.at[r, cut], sibling)

    def tile_at(first, size, column, cut):
        return got_down.at[pl.ds(pl.multiple_of(first, LINE), size), pl.ds(pl.multiple_of(column * width + cut * tile, tile), tile)]

    def split_at(group, column, cut):
        return tile_at(group * part, part, column, cut)

    def shared_at(column, cut):
        return tile_at(groups * part, both, column, cut)

    def down_split(cut):
        here = split_at(y, t, cut)
        return remote(here, here, split_send.at[cut], split_recv.at[cut], across_x)

    def down_shared(cut):
        here = shared_at(t, cut)
        return remote(here, here, shared_send.at[cut], shared_recv.at[cut], across_x)

    def down_y(cut):
        here = split_at(y, other + k, cut)
        return remote(here, here, dy_send.at[cut], dy_recv.at[cut], across_y)

    def down_a(cut):
        here = split_at(y, other + k, cut)
        return remote(here, here, da_send.at[cut], da_recv.at[cut], sibling)

    def down_s(cut):
        here = shared_at(other + k, cut)
        return remote(here, here, ds_send.at[cut], ds_recv.at[cut], sibling)

    def down_b(cut):
        here = split_at(1 - y, other + k, cut)
        return remote(here, here, db_send.at[cut], db_recv.at[cut], sibling)

    own_columns = got_down.at[:, pl.ds(pl.multiple_of(t * width, width), width)]
    down_own = remote(own_columns, own_columns, own_send, own_recv, sibling)

    slab = stage.shape[1]
    slots = stage.shape[0]
    slabs = height // slab

    def take(step):
        return pltpu.make_async_copy(master_ref.at[pl.ds(step * slab, slab), :], stage.at[step % slots], load_down.at[step % slots])

    take_tokens = pltpu.make_async_copy(tokens_ref, rows_ref, load_tokens)

    for cut in range(up_cuts):
        for lane in range(CORES):
            up_load(lane, cut).start()
    for step in range(slots):
        take(step).start()
    take_tokens.start()

    barrier = pltpu.get_barrier_semaphore()
    partners = [sibling, across_y] + [(y, f, other + lane) for lane in range(CORES)]
    partners += [(y, rows_from[j], x * CORES + lane) for j in range(1, fs) for lane in range(CORES)]
    for partner in partners:
        pl.semaphore_signal(barrier, inc=1, device_id=partner, device_id_type=MESH)

    gains[...] = jnp.transpose(jnp.broadcast_to(gain_ref[...], (128, gain_ref.shape[1])))

    def up_cast(cut):
        for lane in range(CORES):
            up_load(lane, cut).wait()

            @pl.loop(0, rows // LINE)
            def _(line):
                at = pl.ds(pl.multiple_of(line * LINE, LINE), LINE)
                scale = gains[pl.ds(pl.multiple_of((y * CORES + lane) * rows + line * LINE, LINE), LINE), :]
                block = up_stage[lane, at, pl.ds(cut * cols, cols)]
                up_src[lane, at, pl.ds(cut * cols, cols)] = (jnp.concatenate([scale] * (cols // 128), axis=1) * block).astype(jnp.bfloat16)

    def up_start(cut):
        for lane in range(CORES):
            @pl.when(t == f)
            def _():
                up_cross_own(lane, cut).start()

            @pl.when(t != f)
            def _():
                up_cross(lane, cut).start()

        for lane in range(CORES):
            @pl.when(jnp.logical_or(t != f, lane != k))
            def _():
                up_home(lane, cut).start()

        @pl.when(t == f)
        def _():
            up_local(cut).start()

    up_cast(0)
    pl.semaphore_wait(barrier, len(partners))
    for cut in range(up_cuts):
        up_start(cut)
        if cut + 1 < up_cuts:
            up_cast(cut + 1)

    for step in range(slabs):
        take(step).wait()

        @pl.loop(0, slab // LINE)
        def _(line):
            start = pl.multiple_of(line * LINE, LINE)
            to = pl.ds(pl.multiple_of(step * slab + start, LINE), LINE)
            got_down[to, pl.ds(pl.multiple_of(t * width, width), width)] = stage[step % slots, pl.ds(start, LINE), :].astype(jnp.bfloat16)

        if step + slots < slabs:
            take(step + slots).start()
    down_own.start()

    take_tokens.wait()

    @pl.loop(0, tokens_ref.shape[0] // LINE)
    def _(step):
        at = pl.ds(pl.multiple_of(step * LINE, LINE), LINE)
        rows_ref[at, :] = normalize(rows_ref[at, :])

    def hidden_units(cut):
        @pl.loop(0, cols // UNIT)
        def _(step):
            at = pl.ds(pl.multiple_of(cut * cols + step * UNIT, UNIT), UNIT)
            block = got_up[:, :, :, at].reshape(depth, UNIT)
            before = jnp.dot(rows_ref[...], block, preferred_element_type=jnp.float32)
            hidden[:, at] = jnp.square(jnp.maximum(before, 0.0)).astype(jnp.bfloat16)

    def up_arrive(j, cut):
        r = rows_from[j]
        up_here(r, cut).wait()
        up_y(r, cut).start()
        up_a(r, cut).start()

    def up_second(j, cut):
        r = rows_from[j]
        up_y(r, cut).wait_recv()
        up_b(r, cut).start()

    def up_done(cut):
        for j in range(fs):
            up_a(rows_from[j], cut).wait_recv()
            up_b(rows_from[j], cut).wait_recv()
        hidden_units(cut)

    waiting, seen, ready = [], [0] * up_cuts, []

    def follow():
        j, cut = waiting.pop(0)
        up_second(j, cut)
        seen[cut] += 1
        if seen[cut] == fs:
            ready.append(cut)

    for kind, j, cut in up_order(fs, up_cuts):
        if kind == "relay":
            for slot in range(CORES):
                @pl.when(other + slot != f)
                def _():
                    relay_here(slot, cut).wait()
                    up_relay(slot, cut).start()
        elif kind == "split":
            for piece in range(down_cuts):
                down_split(piece).start()
        elif kind == "shared":
            for piece in range(down_cuts):
                down_shared(piece).start()
        else:
            up_arrive(j, cut)
            waiting.append((j, cut))
            if len(waiting) > LAG:
                follow()
            elif len(ready) > 1:
                up_done(ready.pop(0))

    for cut in range(down_cuts):
        down_split(cut).wait_recv()
        down_y(cut).start()
        down_a(cut).start()
    while waiting:
        follow()
    while ready:
        up_done(ready.pop(0))

    def sum_near(g, cut):
        at = pl.ds(cut * tile, tile)
        return remote(send1.at[g, :, at], recv1.at[g, :, at], send1_send.at[g, cut], send1_recv.at[g, cut], (y, near, t))

    def sum_far(cut):
        at = pl.ds(cut * tile, tile)
        return remote(send2.at[:, at], recv2.at[:, at], send2_send.at[cut], send2_recv.at[cut], (y, rows_from[2], t))

    bases = (x * CORES, other)
    close = (x == f // CORES, x != f // CORES)

    def term(column, cut):
        at = pl.ds(pl.multiple_of(column * width + cut * tile, tile), tile)
        return jnp.dot(hidden[...], got_down[:, at], preferred_element_type=jnp.float32)

    def features(g, cut):
        at = pl.ds(cut * tile, tile)
        send1[g, :, at] = term(bases[g] + 1 - f % 2, cut).astype(jnp.bfloat16)
        sum_near(g, cut).start()
        keep[g, :, at] = term(bases[g] + f % 2, cut)

    def merge(g, cut):
        at = pl.ds(cut * tile, tile)
        sum_near(g, cut).wait_recv()
        total = keep[g, :, at] + recv1[g, :, at].astype(jnp.float32)

        @pl.when(close[g])
        def _():
            keep[g, :, at] = total

        @pl.when(jnp.logical_not(close[g]))
        def _():
            send2[:, at] = total.astype(jnp.bfloat16)
            sum_far(cut).start()

    def finish(cut):
        at = pl.ds(cut * tile, tile)
        sum_far(cut).wait_recv()
        total = keep[(x + f // CORES) % PLANES, :, at] + recv2[:, at].astype(jnp.float32)
        out_ref[:, at] = total.astype(jnp.bfloat16)

    down_own.wait_recv()
    for step in range(down_cuts + 3):
        if step < down_cuts:
            features(0, step)
            down_shared(step).wait_recv()
            down_s(step).start()
            down_y(step).wait_recv()
            down_b(step).start()
        if 1 <= step <= down_cuts:
            cut = step - 1
            down_a(cut).wait_recv()
            down_s(cut).wait_recv()
            down_b(cut).wait_recv()
            features(1, cut)
            merge(0, cut)
        if 2 <= step <= down_cuts + 1:
            merge(1, step - 2)
        if step >= 3:
            finish(step - 3)

    for cut in range(up_cuts):
        for lane in range(CORES):
            up_cross(lane, cut).wait_send()

            @pl.when(jnp.logical_or(t != f, lane != k))
            def _():
                up_home(lane, cut).wait_send()

        for slot in range(CORES):
            @pl.when(other + slot != f)
            def _():
                up_relay(slot, cut).wait_send()
        for j in range(fs):
            up_y(rows_from[j], cut).wait_send()
            up_a(rows_from[j], cut).wait_send()
            up_b(rows_from[j], cut).wait_send()
    down_own.wait_send()
    for cut in range(down_cuts):
        down_split(cut).wait_send()
        down_shared(cut).wait_send()
        down_y(cut).wait_send()
        down_a(cut).wait_send()
        down_s(cut).wait_send()
        down_b(cut).wait_send()
        sum_near(0, cut).wait_send()
        sum_near(1, cut).wait_send()
        sum_far(cut).wait_send()


def fused(tokens_in, up_master, down_master, norm_gain, dims):
    groups, fs, tp = dims
    rows, cols = up_master.shape[0] // (groups * CORES), up_master.shape[1]
    height, width = down_master.shape
    tokens = tokens_in.shape[0]
    up_cuts = pieces_of(cols, UNIT, UP_CUTS)
    down_cuts = pieces_of(width, 128, DOWN_CUTS)
    slabs = pieces_of(height, LINE, 8)
    dma = pltpu.SemaphoreType.DMA
    lanes, whole, strip = dma((CORES, up_cuts)), dma((fs, up_cuts)), dma((down_cuts,))
    up_sems = [lanes, lanes, whole, lanes, lanes] + [whole] * 6
    down_sems = [dma, dma] + [strip] * 12
    sum_sems = [dma((2, down_cuts)), dma((2, down_cuts)), strip, strip]
    vmem = pl.BlockSpec(memory_space=pltpu.VMEM)
    hbm = pl.BlockSpec(memory_space=pl.ANY)
    got_up, got_down, out = pl.pallas_call(
        functools.partial(hand_over, dims, (up_cuts, down_cuts)),
        out_shape=(
            pltpu.VMEM((fs, groups * CORES, rows, cols), jnp.bfloat16),
            pltpu.VMEM((height, tp * width), jnp.bfloat16),
            jax.ShapeDtypeStruct((tokens, width), jnp.bfloat16),
        ),
        in_specs=[hbm, vmem, hbm, hbm],
        out_specs=(vmem, vmem, vmem),
        scratch_shapes=[
            pltpu.VMEM(tokens_in.shape, jnp.bfloat16),
            pltpu.VMEM((up_master.shape[0], 128), jnp.float32),
            pltpu.VMEM((CORES, rows, cols), jnp.float32),
            pltpu.VMEM((CORES, rows, cols), jnp.bfloat16),
            pltpu.VMEM((CORES, rows, cols), jnp.bfloat16),
            pltpu.VMEM((2, height // slabs, width), jnp.float32),
            pltpu.VMEM((tokens, cols), jnp.bfloat16),
            pltpu.VMEM((2, tokens, width), jnp.float32),
            pltpu.VMEM((2, tokens, width), jnp.bfloat16),
            pltpu.VMEM((2, tokens, width), jnp.bfloat16),
            pltpu.VMEM((tokens, width), jnp.bfloat16),
            pltpu.VMEM((tokens, width), jnp.bfloat16),
            up_sems,
            down_sems,
            sum_sems,
            [lanes, dma((2,)), dma],
        ],
        compiler_params=pltpu.CompilerParams(collective_id=0, has_side_effects=True, vmem_limit_bytes=LIMIT << 20),
    )(tokens_in, norm_gain.reshape(1, -1), up_master.reshape(groups * CORES, rows, cols), down_master)
    return out, got_up.reshape(fs * groups * CORES * rows, cols), got_down


def fits(up_shape, down_shape, dims):
    groups, fs, tp = dims
    own = 2 * (up_shape[0] * up_shape[1] * fs + down_shape[0] * down_shape[1] * tp)
    aligned = up_shape[0] % (groups * CORES * LINE) == 0 and up_shape[0] % 128 == 0 and up_shape[1] % UNIT == 0
    square = groups == 2 and tp == CORES * PLANES and fs == tp
    return square and aligned and down_shape[0] % (groups * LINE) == 0 and down_shape[1] % 128 == 0 and own <= 40 << 20


def by_collectives(normalized, up_cast, down_cast):
    quarter = lax.all_to_all(up_cast, "tp", split_axis=0, concat_axis=1, tiled=True)
    moved = lax.all_to_all(quarter, "fs", split_axis=1, concat_axis=0, tiled=True)
    part_rows = quarter.shape[0]
    stacked = moved.reshape(moved.shape[0] // part_rows, part_rows, moved.shape[1])
    joined = lax.all_gather(stacked, "tp", axis=1, tiled=True)
    sampled_down = lax.all_gather(down_cast, "tp", axis=1, tiled=True)
    sampled_up = joined.reshape(joined.shape[0] * joined.shape[1], joined.shape[2])
    before = jnp.dot(normalized, sampled_up, preferred_element_type=jnp.float32)
    hidden = jnp.square(jax.nn.relu(before)).astype(jnp.bfloat16)
    terms = jnp.dot(hidden, sampled_down, preferred_element_type=jnp.float32)
    summed = lax.psum_scatter(terms, "fs", scatter_dimension=1, tiled=True)
    return summed.astype(jnp.bfloat16), sampled_up, sampled_down


def shards(dims, tokens, up_master, down_master, norm_gain):
    if fits(up_master.shape, down_master.shape, dims):
        return fused(tokens, up_master, down_master, norm_gain, dims)
    up_cast = (norm_gain[:, None] * up_master).astype(jnp.bfloat16)
    return by_collectives(normalize(tokens), up_cast, down_master.astype(jnp.bfloat16))


def solution(mesh):
    dims = tuple(mesh.shape[name] for name in ("grp", "fs", "tp"))
    return jax.shard_map(
        functools.partial(shards, dims),
        mesh=mesh,
        in_specs=(P(("grp", "tp"), None), P("fs", "tp"), P("fs", "tp"), P("fs")),
        out_specs=(P(("grp", "tp"), "fs"), P("grp", "fs"), P(("grp", "fs"), None)),
        check_vma=False,
    )
```

time: 237 us -> 217 us (0.916)
  Pallas kernels: 215 us -> 200 us
  other arithmetic: 7.3 us -> 0 us
    pallas_call x1, Pallas kernels: 215 us -> 200 us  [fused(): pl.pallas_call(functools.partial(hand_over, dims, (up_cuts, down_cuts)),...]
    convert_element_type x1 -> x0, other arithmetic: 7.3 us -> none  [shards(): up_cast = (norm_gain[:, None] * up_master).astype(jnp.bfloat16)]
where the time goes in v1:
time: 217 us; the launch traced here: 216 us
  Pallas kernels  200 us (92%)
  local copies, waits for them, and re-layouts  15.7 us (7%)
    pallas_call x1, Pallas kernels, fused(): pl.pallas_call(functools.partial(hand_over, dims, (up_cuts, down_cuts)),...  200 us
    unnamed x5, local copies, waits for them, and re-layouts  14.5 us

profile of v1, /device:TPU:3, one launch (start us, length us, event | category | flops | bytes accessed | tf_op | source)
XLA Modules:
  0.0 216.3 jit_solution(16803657962550300193)
XLA Ops:
  0.6 1.3 reshape.15.gain_ref
  1.9 200.0 %shard_map.67 = (bf16[4,4,192,3072]{3,2,1,0:T(8,128)(2,1)S(1)}, bf16[3072,3072]{1,0:T(8,128)(2,1)S(1)}, bf16[256,768]{1,0:T(8,128)(2,1)}) custom-call(bf16[256,3072]{1,0:T(8,128)(2,1)} %tokens_ref.1, f32[1,768]{1,0:T(1,128)} %reshape.15.gain_ref, f32[4,192,3072]{2,1,0:T(8,128)} %bitcast.3, f32[3072,768]{1,0:T(8,128)} %master_ref.1), custom_call_target="tpu_custom_call" | custom-call | tf_op jit(solution)/shard_map/pallas_call | solution.py:408
  201.9 6.9 %copy.10 = bf16[3072,3072]{1,0:T(8,128)(2,1)} copy(bf16[3072,3072]{1,0:T(8,128)(2,1)S(1)} %bitcast.2) | data formatting | bytes 37748736
  208.7 0.0 copy-start
  208.7 6.8 %copy.11 = bf16[3072,3072]{1,0:T(8,128)(2,1)} copy(bf16[3072,3072]{1,0:T(8,128)(2,1)S(1)} %get-tuple-element.11) | data formatting | bytes 37748736
  215.6 0.0 copy-done
  215.6 0.7 copy.12
Async XLA Ops:
  208.7 6.9 %copy-start = (bf16[256,768]{1,0:T(8,128)(2,1)S(1)}, bf16[256,768]{1,0:T(8,128)(2,1)}, u32[]{:S(2)}) copy-start(bf16[256,768]{1,0:T(8,128)(2,1)} %get-tuple-element.15) | copy-start | bytes 1179652

commit v2 on v1

--- a/solution.py
+++ b/solution.py
@@ -14,9 +14,10 @@
 UNIT = 256
 LINE = 16
 LIMIT = 24
+START = 0.15
 UP_CUTS = 6
 DOWN_CUTS = 6
-SHARED = 8
+SHARED = 9
 SHARES = 16
 
 
@@ -38,17 +39,32 @@
     return height * SHARED // SHARES // (2 * LINE) * (2 * LINE)
 
 
-def up_order(fs, cuts):
-    events = []
-    for cut in range(cuts):
-        at = (cut + 1) / cuts
-        events.append((at, 0, "relay", 0, cut))
-        for j in range(fs):
-            pace = (1.0, 1.25, 2.0, 2.0)[j]
-            events.append((at * pace, 1 + j, "arrive", j, cut))
-    events.append((0.55, 9, "split", 0, 0))
-    events.append((0.85, 9, "shared", 0, 0))
-    return [event[2:] for event in sorted(events)]
+def order_of(fs, up_cuts, down_cuts, share):
+    ready = []
+    for cut in range(up_cuts):
+        at = (cut + 1) / up_cuts
+        ready.append((START + at, 0, "relay", 0, cut))
+        for j, came in enumerate((START + at, START + 0.1 + 1.5 * at, START + 0.2 + 1.5 * at, START + 1.15 + at)):
+            ready.append((came, 1, "arrive", j, cut))
+    for cut in range(down_cuts):
+        at = (cut + 1) / down_cuts
+        ready.append((START + 1.05 + (1 - share) * at, 2, "split", 0, cut))
+        ready.append((START + 1.05 + 1 - share + 2 * share * at, 4, "shared", 0, cut))
+    ready.append((START + 0.3, 0, "send", 0, 0))
+    ready.append((START + 0.6, 0, "send", 1, 0))
+    ready.sort()
+    order, spare, now = [], [], START
+    for came, _, kind, j, cut in ready:
+        while spare and kind == "arrive" and now + (1 - share) / down_cuts <= came:
+            order.append(("cross", 0, spare.pop(0)))
+            now += (1 - share) / down_cuts
+        order.append((kind, j, cut))
+        if kind == "arrive":
+            now = max(now, came) + 2 / (fs * up_cuts)
+        if kind == "split":
+            spare.append(cut)
+    last = max(i for i, entry in enumerate(order) if entry[0] == "arrive") + 1
+    return order[:last], spare
 
 
 def hand_over(dims, cuts, tokens_ref, gain_ref, up_ref, master_ref, got_up, got_down, out_ref, rows_ref, gains, up_stage, up_src, relayed, stage, hidden, keep, send1, recv1, send2, recv2, up_sems, down_sems, sum_sems, load_sems):
@@ -67,7 +83,8 @@
     both = shared_rows(height)
     part = (height - both) // groups
     near = f + 1 - 2 * (f % 2)
-    rows_from = (f, near, (f + 2) % fs, (near + 2) % fs)
+    rows_from = (f, near, (fs - 1) * (1 - f // 2), 2 - f // 2)
+    facing = (f + 2) % fs
     sibling = (y, f, x * CORES + (1 - k))
     across_y = (1 - y, f, t)
     other = (1 - x) * CORES
@@ -177,7 +194,7 @@
     for partner in partners:
         pl.semaphore_signal(barrier, inc=1, device_id=partner, device_id_type=MESH)
 
-    gains[...] = jnp.transpose(jnp.broadcast_to(gain_ref[...], (128, gain_ref.shape[1])))
+    gains[...] = jnp.transpose(jnp.broadcast_to(gain_ref[...][None, :], (128, gain_ref.shape[0])))
 
     def up_cast(cut):
         for lane in range(CORES):
@@ -200,6 +217,7 @@
             def _():
                 up_cross(lane, cut).start()
 
+    def up_direct(cut):
         for lane in range(CORES):
             @pl.when(jnp.logical_or(t != f, lane != k))
             def _():
@@ -209,12 +227,13 @@
         def _():
             up_local(cut).start()
 
-    up_cast(0)
+    for cut in range(up_cuts):
+        up_cast(cut)
     pl.semaphore_wait(barrier, len(partners))
     for cut in range(up_cuts):
         up_start(cut)
-        if cut + 1 < up_cuts:
-            up_cast(cut + 1)
+        if cut == 0:
+            up_direct(cut)
 
     for step in range(slabs):
         take(step).wait()
@@ -261,105 +280,138 @@
             up_b(rows_from[j], cut).wait_recv()
         hidden_units(cut)
 
-    waiting, seen, ready = [], [0] * up_cuts, []
+    def sum_near(g, cut):
+        at = pl.ds(cut * tile, tile)
+        return remote(send1.at[g, :, at], recv1.at[g, :, at], send1_send.at[g, cut], send1_recv.at[g, cut], (y, near, t))
+
+    def sum_far(cut):
+        at = pl.ds(cut * tile, tile)
+        return remote(send2.at[:, at], recv2.at[:, at], send2_send.at[cut], send2_recv.at[cut], (y, facing, t))
+
+    bases = (x * CORES, other)
+    close = (x == f // CORES, x != f // CORES)
+
+    def features(g, cut):
+        at = pl.ds(cut * tile, tile)
+        other_at, here_at = (pl.ds(pl.multiple_of(column * width + cut * tile, tile), tile) for column in (bases[g] + 1 - f % 2, bases[g] + f % 2))
+        both_terms = jnp.zeros((hidden.shape[0], 2 * tile), jnp.float32)
+        for unit in range(0, height, UNIT):
+            rows_at = pl.ds(unit, UNIT)
+            block = jnp.concatenate([got_down[rows_at, other_at], got_down[rows_at, here_at]], axis=1)
+            both_terms += jnp.dot(hidden[:, rows_at], block, preferred_element_type=jnp.float32)
+        send1[g, :, at] = both_terms[:, :tile].astype(jnp.bfloat16)
+        sum_near(g, cut).start()
+        keep[g, :, at] = both_terms[:, tile:]
+
+    def merge(g, cut):
+        at = pl.ds(cut * tile, tile)
+        sum_near(g, cut).wait_recv()
+        total = keep[g, :, at] + recv1[g, :, at].astype(jnp.float32)
+
+        @pl.when(close[g])
+        def _():
+            keep[g, :, at] = total
+
+        @pl.when(jnp.logical_not(close[g]))
+        def _():
+            send2[:, at] = total.astype(jnp.bfloat16)
+            sum_far(cut).start()
+
+    def finish(cut):
+        at = pl.ds(cut * tile, tile)
+        sum_far(cut).wait_recv()
+        total = keep[(x + f // CORES) % PLANES, :, at] + recv2[:, at].astype(jnp.float32)
+        out_ref[:, at] = total.astype(jnp.bfloat16)
+
+    waiting, seen, ready, crossed, shared = [], [0] * up_cuts, [], [], []
 
     def follow():
-        j, cut = waiting.pop(0)
-        up_second(j, cut)
-        seen[cut] += 1
-        if seen[cut] == fs:
-            ready.append(cut)
-
-    for kind, j, cut in up_order(fs, up_cuts):
+        kind, j, cut = waiting.pop(0)
+        if kind == "cross":
+            down_y(cut).wait_recv()
+            down_b(cut).start()
+            crossed.append(cut)
+        else:
+            up_second(j, cut)
+            seen[cut] += 1
+            if seen[cut] == fs:
+                ready.append(cut)
+
+    def shared_in(cut):
+        down_shared(cut).wait_recv()
+        down_s(cut).start()
+        shared.append(cut)
+
+    order, late = order_of(fs, up_cuts, down_cuts, both / height)
+    for kind, j, cut in order:
         if kind == "relay":
             for slot in range(CORES):
                 @pl.when(other + slot != f)
                 def _():
                     relay_here(slot, cut).wait()
                     up_relay(slot, cut).start()
+
+            if cut + 1 < up_cuts:
+                up_direct(cut + 1)
+        elif kind == "send":
+            for piece in range(down_cuts):
+                (down_split, down_shared)[j](piece).start()
         elif kind == "split":
-            for piece in range(down_cuts):
-                down_split(piece).start()
+            down_split(cut).wait_recv()
+            down_a(cut).start()
         elif kind == "shared":
-            for piece in range(down_cuts):
-                down_shared(piece).start()
+            shared_in(cut)
         else:
-            up_arrive(j, cut)
-            waiting.append((j, cut))
+            if kind == "cross":
+                down_y(cut).start()
+            else:
+                up_arrive(j, cut)
+            waiting.append((kind, j, cut))
             if len(waiting) > LAG:
                 follow()
-            elif len(ready) > 1:
+            if len(ready) > 1:
                 up_done(ready.pop(0))
 
+    for cut in late:
+        down_y(cut).start()
+        waiting.append(("cross", 0, cut))
+    while sum(seen) < fs * up_cuts:
+        follow()
+        while ready:
+            up_done(ready.pop(0))
+    down_own.wait_recv()
+
+    merging, merged, paired = [], [0] * down_cuts, 0
+
+    def settle(limit):
+        while len(merging) > limit:
+            g, cut = merging.pop(0)
+            merge(g, cut)
+            merged[cut] += 1
+
+    for step in range(down_cuts):
+        features(0, step)
+        merging.append((0, step))
+        if step % 2 == 1:
+            if waiting:
+                follow()
+            settle(3)
+    while paired < down_cuts:
+        if len(shared) < down_cuts and len(shared) <= len(crossed):
+            shared_in(len(shared))
+        if waiting:
+            follow()
+        if paired + 1 < len(crossed) or not waiting:
+            down_a(paired).wait_recv()
+            down_s(paired).wait_recv()
+            down_b(paired).wait_recv()
+            features(1, paired)
+            merging.append((1, paired))
+            paired += 1
+        settle(2)
+    settle(0)
     for cut in range(down_cuts):
-        down_split(cut).wait_recv()
-        down_y(cut).start()
-        down_a(cut).start()
-    while waiting:
-        follow()
-    while ready:
-        up_done(ready.pop(0))
-
-    def sum_near(g, cut):
-        at = pl.ds(cut * tile, tile)
-        return remote(send1.at[g, :, at], recv1.at[g, :, at], send1_send.at[g, cut], send1_recv.at[g, cut], (y, near, t))
-
-    def sum_far(cut):
-        at = pl.ds(cut * tile, tile)
-        return remote(send2.at[:, at], recv2.at[:, at], send2_send.at[cut], send2_recv.at[cut], (y, rows_from[2], t))
-
-    bases = (x * CORES, other)
-    close = (x == f // CORES, x != f // CORES)
-
-    def term(column, cut):
-        at = pl.ds(pl.multiple_of(column * width + cut * tile, tile), tile)
-        return jnp.dot(hidden[...], got_down[:, at], preferred_element_type=jnp.float32)
-
-    def features(g, cut):
-        at = pl.ds(cut * tile, tile)
-        send1[g, :, at] = term(bases[g] + 1 - f % 2, cut).astype(jnp.bfloat16)
-        sum_near(g, cut).start()
-        keep[g, :, at] = term(bases[g] + f % 2, cut)
-
-    def merge(g, cut):
-        at = pl.ds(cut * tile, tile)
-        sum_near(g, cut).wait_recv()
-        total = keep[g, :, at] + recv1[g, :, at].astype(jnp.float32)
-
-        @pl.when(close[g])
-        def _():
-            keep[g, :, at] = total
-
-        @pl.when(jnp.logical_not(close[g]))
-        def _():
-            send2[:, at] = total.astype(jnp.bfloat16)
-            sum_far(cut).start()
-
-    def finish(cut):
-        at = pl.ds(cut * tile, tile)
-        sum_far(cut).wait_recv()
-        total = keep[(x + f // CORES) % PLANES, :, at] + recv2[:, at].astype(jnp.float32)
-        out_ref[:, at] = total.astype(jnp.bfloat16)
-
-    down_own.wait_recv()
-    for step in range(down_cuts + 3):
-        if step < down_cuts:
-            features(0, step)
-            down_shared(step).wait_recv()
-            down_s(step).start()
-            down_y(step).wait_recv()
-            down_b(step).start()
-        if 1 <= step <= down_cuts:
-            cut = step - 1
-            down_a(cut).wait_recv()
-            down_s(cut).wait_recv()
-            down_b(cut).wait_recv()
-            features(1, cut)
-            merge(0, cut)
-        if 2 <= step <= down_cuts + 1:
-            merge(1, step - 2)
-        if step >= 3:
-            finish(step - 3)
+        finish(cut)
 
     for cut in range(up_cuts):
         for lane in range(CORES):
@@ -433,7 +485,7 @@
             [lanes, dma((2,)), dma],
         ],
         compiler_params=pltpu.CompilerParams(collective_id=0, has_side_effects=True, vmem_limit_bytes=LIMIT << 20),
-    )(tokens_in, norm_gain.reshape(1, -1), up_master.reshape(groups * CORES, rows, cols), down_master)
+    )(tokens_in, norm_gain, up_master.reshape(groups * CORES, rows, cols), down_master)
     return out, got_up.reshape(fs * groups * CORES * rows, cols), got_down
 
 
@@ -442,7 +494,7 @@
     own = 2 * (up_shape[0] * up_shape[1] * fs + down_shape[0] * down_shape[1] * tp)
     aligned = up_shape[0] % (groups * CORES * LINE) == 0 and up_shape[0] % 128 == 0 and up_shape[1] % UNIT == 0
     square = groups == 2 and tp == CORES * PLANES and fs == tp
-    return square and aligned and down_shape[0] % (groups * LINE) == 0 and down_shape[1] % 128 == 0 and own <= 40 << 20
+    return square and aligned and down_shape[0] % UNIT == 0 and down_shape[1] % 128 == 0 and own <= 40 << 20
 
 
 def by_collectives(normalized, up_cast, down_cast):

time: 217 us -> 179 us (0.82)
  Pallas kernels: 200 us -> 164 us
    pallas_call x1, Pallas kernels: 200 us -> 164 us  [fused(): pl.pallas_call(functools.partial(hand_over, dims, (up_cuts, down_cuts)),...]
where the time goes in v2:
time: 179 us
  Pallas kernels  164 us (92%)
  local copies, waits for them, and re-layouts  14.5 us (8%)
    pallas_call x1, Pallas kernels, fused(): pl.pallas_call(functools.partial(hand_over, dims, (up_cuts, down_cuts)),...  164 us
    unnamed x5, local copies, waits for them, and re-layouts  14.5 us

profile of v2, /device:TPU:3, one launch (start us, length us, event | category | flops | bytes accessed | tf_op | source)
XLA Modules:
  0.0 178.8 jit_solution(9071942975868985708)
XLA Ops:
  0.6 163.7 %shard_map.67 = (bf16[4,4,192,3072]{3,2,1,0:T(8,128)(2,1)S(1)}, bf16[3072,3072]{1,0:T(8,128)(2,1)S(1)}, bf16[256,768]{1,0:T(8,128)(2,1)}) custom-call(bf16[256,3072]{1,0:T(8,128)(2,1)} %tokens_ref.1, f32[768]{0:T(1024)} %gain_ref.1, f32[4,192,3072]{2,1,0:T(8,128)} %bitcast.3, f32[3072,768]{1,0:T(8,128)} %master_ref.1), custom_call_target="tpu_custom_call" | custom-call | tf_op jit(solution)/shard_map/pallas_call | solution.py:460
  164.3 6.9 %copy.10 = bf16[3072,3072]{1,0:T(8,128)(2,1)} copy(bf16[3072,3072]{1,0:T(8,128)(2,1)S(1)} %bitcast.2) | data formatting | bytes 37748736
  171.2 0.0 copy-start
  171.2 6.8 %copy.11 = bf16[3072,3072]{1,0:T(8,128)(2,1)} copy(bf16[3072,3072]{1,0:T(8,128)(2,1)S(1)} %get-tuple-element.11) | data formatting | bytes 37748736
  178.0 0.0 copy-done
  178.0 0.7 copy.12
Async XLA Ops:
  171.2 6.9 %copy-start = (bf16[256,768]{1,0:T(8,128)(2,1)S(1)}, bf16[256,768]{1,0:T(8,128)(2,1)}, u32[]{:S(2)}) copy-start(bf16[256,768]{1,0:T(8,128)(2,1)} %get-tuple-element.15) | copy-start | bytes 1179652

commit v3 on v2

--- a/solution.py
+++ b/solution.py
@@ -14,11 +14,15 @@
 UNIT = 256
 LINE = 16
 LIMIT = 24
-START = 0.15
-UP_CUTS = 6
+STAGES = 4
+DELAY = 3
+AHEAD = 2
+NORMS = 4
+START = 0.12
+UP_CUTS = 12
 DOWN_CUTS = 6
-SHARED = 9
-SHARES = 16
+SHARED = 19
+SHARES = 32
 
 
 def normalize(tokens):
@@ -67,13 +71,13 @@
     return order[:last], spare
 
 
-def hand_over(dims, cuts, tokens_ref, gain_ref, up_ref, master_ref, got_up, got_down, out_ref, rows_ref, gains, up_stage, up_src, relayed, stage, hidden, keep, send1, recv1, send2, recv2, up_sems, down_sems, sum_sems, load_sems):
+def hand_over(dims, cuts, tokens_ref, gain_ref, up_ref, master_ref, got_up, got_down, out_ref, rows_ref, gains, up_stage, up_src, relayed, stage, hidden, hold, keep, send1, recv1, send2, recv2, up_sems, down_sems, sum_sems, load_sems):
     groups, fs, tp = dims
     up_cuts, down_cuts = cuts
     y, f, t = lax.axis_index("grp"), lax.axis_index("fs"), lax.axis_index("tp")
     x, k = t // CORES, t % CORES
-    home_send, cross_send, first_recv, relay_send, relay_recv, y_send, y_recv, a_send, a_recv, b_send, b_recv = up_sems
-    own_send, own_recv, split_send, split_recv, shared_send, shared_recv, dy_send, dy_recv, da_send, da_recv, ds_send, ds_recv, db_send, db_recv = down_sems
+    home_send, cross_send, relay_send, y_send, a_send, b_send, first_recv, relay_recv, y_recv, pair_recv = up_sems
+    own_send, own_recv, split_send, shared_send, dy_send, da_send, ds_send, db_send, split_recv, shared_recv, dy_recv, twin_recv = down_sems
     send1_send, send1_recv, send2_send, send2_recv = sum_sems
     load_up, load_down, load_tokens = load_sems
     rows, cols = up_src.shape[1], up_src.shape[2] // up_cuts
@@ -101,22 +105,22 @@
 
     def up_load(lane, cut):
         at = pl.ds(cut * cols, cols)
-        return pltpu.make_async_copy(up_ref.at[y * CORES + lane, :, at], up_stage.at[lane, :, at], load_up.at[lane, cut])
+        return pltpu.make_async_copy(up_ref.at[y * CORES + lane, :, at], up_stage.at[lane, :, at], load_up.at[cut])
 
     def up_local(cut):
         return pltpu.make_async_copy(src_at(k, cut), up_at(got_up.at[f], y, k, cut), first_recv.at[f, cut])
 
     def up_home(lane, cut):
-        return remote(src_at(lane, cut), up_at(got_up.at[f], y, lane, cut), home_send.at[lane, cut], first_recv.at[f, cut], (y, t, x * CORES + lane))
+        return remote(src_at(lane, cut), up_at(got_up.at[f], y, lane, cut), home_send, first_recv.at[f, cut], (y, t, x * CORES + lane))
 
     def up_cross_own(lane, cut):
-        return remote(src_at(lane, cut), up_at(got_up.at[f], y, lane, cut), cross_send.at[lane, cut], first_recv.at[f, cut], (y, f, other + lane))
+        return remote(src_at(lane, cut), up_at(got_up.at[f], y, lane, cut), cross_send, first_recv.at[f, cut], (y, f, other + lane))
 
     def up_cross(lane, cut):
-        return remote(src_at(lane, cut), relayed.at[k, :, pl.ds(cut * cols, cols)], cross_send.at[lane, cut], relay_recv.at[k, cut], (y, f, other + lane))
+        return remote(src_at(lane, cut), relayed.at[k, :, pl.ds(cut * cols, cols)], cross_send, relay_recv.at[k, cut], (y, f, other + lane))
 
     def up_relay(slot, cut):
-        return remote(relayed.at[slot, :, pl.ds(cut * cols, cols)], up_at(got_up.at[f], y, k, cut), relay_send.at[slot, cut], first_recv.at[f, cut], (y, other + slot, t))
+        return remote(relayed.at[slot, :, pl.ds(cut * cols, cols)], up_at(got_up.at[f], y, k, cut), relay_send, first_recv.at[f, cut], (y, other + slot, t))
 
     def up_here(r, cut):
         return pltpu.make_async_copy(src_at(0, cut), up_at(got_up.at[r], y, k, cut), first_recv.at[r, cut])
@@ -126,15 +130,15 @@
 
     def up_y(r, cut):
         here = up_at(got_up.at[r], y, k, cut)
-        return remote(here, here, y_send.at[r, cut], y_recv.at[r, cut], across_y)
+        return remote(here, here, y_send, y_recv.at[r, cut], across_y)
 
     def up_a(r, cut):
         here = up_at(got_up.at[r], y, k, cut)
-        return remote(here, here, a_send.at[r, cut], a_recv.at[r, cut], sibling)
+        return remote(here, here, a_send, pair_recv.at[cut], sibling)
 
     def up_b(r, cut):
         here = up_at(got_up.at[r], 1 - y, k, cut)
-        return remote(here, here, b_send.at[r, cut], b_recv.at[r, cut], sibling)
+        return remote(here, here, b_send, pair_recv.at[cut], sibling)
 
     def tile_at(first, size, column, cut):
         return got_down.at[pl.ds(pl.multiple_of(first, LINE), size), pl.ds(pl.multiple_of(column * width + cut * tile, tile), tile)]
@@ -147,27 +151,27 @@
 
     def down_split(cut):
         here = split_at(y, t, cut)
-        return remote(here, here, split_send.at[cut], split_recv.at[cut], across_x)
+        return remote(here, here, split_send, split_recv.at[cut], across_x)
 
     def down_shared(cut):
         here = shared_at(t, cut)
-        return remote(here, here, shared_send.at[cut], shared_recv.at[cut], across_x)
+        return remote(here, here, shared_send, shared_recv.at[cut], across_x)
 
     def down_y(cut):
         here = split_at(y, other + k, cut)
-        return remote(here, here, dy_send.at[cut], dy_recv.at[cut], across_y)
+        return remote(here, here, dy_send, dy_recv.at[cut], across_y)
 
     def down_a(cut):
         here = split_at(y, other + k, cut)
-        return remote(here, here, da_send.at[cut], da_recv.at[cut], sibling)
+        return remote(here, here, da_send, twin_recv.at[cut], sibling)
 
     def down_s(cut):
         here = shared_at(other + k, cut)
-        return remote(here, here, ds_send.at[cut], ds_recv.at[cut], sibling)
+        return remote(here, here, ds_send, twin_recv.at[cut], sibling)
 
     def down_b(cut):
         here = split_at(1 - y, other + k, cut)
-        return remote(here, here, db_send.at[cut], db_recv.at[cut], sibling)
+        return remote(here, here, db_send, twin_recv.at[cut], sibling)
 
     own_columns = got_down.at[:, pl.ds(pl.multiple_of(t * width, width), width)]
     down_own = remote(own_columns, own_columns, own_send, own_recv, sibling)
@@ -197,9 +201,9 @@
     gains[...] = jnp.transpose(jnp.broadcast_to(gain_ref[...][None, :], (128, gain_ref.shape[0])))
 
     def up_cast(cut):
+        whole = up_stage.at[:, :, pl.ds(cut * cols, cols)]
+        pltpu.make_async_copy(whole, whole, load_up.at[cut]).wait()
         for lane in range(CORES):
-            up_load(lane, cut).wait()
-
             @pl.loop(0, rows // LINE)
             def _(line):
                 at = pl.ds(pl.multiple_of(line * LINE, LINE), LINE)
@@ -235,7 +239,7 @@
         if cut == 0:
             up_direct(cut)
 
-    for step in range(slabs):
+    def down_cast(step):
         take(step).wait()
 
         @pl.loop(0, slab // LINE)
@@ -246,14 +250,18 @@
 
         if step + slots < slabs:
             take(step + slots).start()
-    down_own.start()
-
-    take_tokens.wait()
-
-    @pl.loop(0, tokens_ref.shape[0] // LINE)
-    def _(step):
-        at = pl.ds(pl.multiple_of(step * LINE, LINE), LINE)
-        rows_ref[at, :] = normalize(rows_ref[at, :])
+        if step == slabs - 1:
+            down_own.start()
+
+    def normalize_rows(step):
+        if step == 0:
+            take_tokens.wait()
+        span = tokens_ref.shape[0] // NORMS
+
+        @pl.loop(0, span // LINE)
+        def _(line):
+            at = pl.ds(pl.multiple_of(step * span + line * LINE, LINE), LINE)
+            rows_ref[at, :] = normalize(rows_ref[at, :])
 
     def hidden_units(cut):
         @pl.loop(0, cols // UNIT)
@@ -275,55 +283,111 @@
         up_b(r, cut).start()
 
     def up_done(cut):
-        for j in range(fs):
-            up_a(rows_from[j], cut).wait_recv()
-            up_b(rows_from[j], cut).wait_recv()
+        landed = got_up.at[:, pl.ds(0, groups), :, pl.ds(cut * cols, cols)]
+        pltpu.make_async_copy(landed, landed, pair_recv.at[cut]).wait()
         hidden_units(cut)
 
     def sum_near(g, cut):
         at = pl.ds(cut * tile, tile)
-        return remote(send1.at[g, :, at], recv1.at[g, :, at], send1_send.at[g, cut], send1_recv.at[g, cut], (y, near, t))
+        return remote(send1.at[g, :, at], recv1.at[g, :, at], send1_send, send1_recv.at[g, cut], (y, near, t))
 
     def sum_far(cut):
         at = pl.ds(cut * tile, tile)
-        return remote(send2.at[:, at], recv2.at[:, at], send2_send.at[cut], send2_recv.at[cut], (y, facing, t))
+        return remote(send2.at[:, at], recv2.at[:, at], send2_send, send2_recv.at[cut], (y, facing, t))
 
     bases = (x * CORES, other)
-    close = (x == f // CORES, x != f // CORES)
-
-    def features(g, cut):
+    close = x == f // CORES
+    kept = (x + f // CORES) % PLANES
+
+    def terms(g, cut, first, last):
+        away, here = (pl.ds(pl.multiple_of(column * width + cut * tile, tile), tile) for column in (bases[g] + 1 - f % 2, bases[g] + f % 2))
+        total = jnp.zeros((hidden.shape[0], 2 * tile), jnp.float32)
+        for unit in range(first, last, UNIT):
+            at = pl.ds(unit, UNIT)
+            block = jnp.concatenate([got_down[at, away], got_down[at, here]], axis=1)
+            total += jnp.dot(hidden[:, at], block, preferred_element_type=jnp.float32)
+        return total[:, :tile], total[:, tile:]
+
+    def features(g, cut, first, last):
         at = pl.ds(cut * tile, tile)
-        other_at, here_at = (pl.ds(pl.multiple_of(column * width + cut * tile, tile), tile) for column in (bases[g] + 1 - f % 2, bases[g] + f % 2))
-        both_terms = jnp.zeros((hidden.shape[0], 2 * tile), jnp.float32)
-        for unit in range(0, height, UNIT):
-            rows_at = pl.ds(unit, UNIT)
-            block = jnp.concatenate([got_down[rows_at, other_at], got_down[rows_at, here_at]], axis=1)
-            both_terms += jnp.dot(hidden[:, rows_at], block, preferred_element_type=jnp.float32)
-        send1[g, :, at] = both_terms[:, :tile].astype(jnp.bfloat16)
-        sum_near(g, cut).start()
-        keep[g, :, at] = both_terms[:, tile:]
-
-    def merge(g, cut):
+        away, here = terms(g, cut, first, last)
+        if first > 0:
+            away, here = hold[:, at] + away, keep[g, :, at] + here
+        keep[g, :, at] = here
+        if last == height:
+            send1[g, :, at] = away.astype(jnp.bfloat16)
+            if g == 1 or cut < AHEAD:
+                sum_near(g, cut).start()
+            else:
+                @pl.when(jnp.logical_not(close))
+                def _():
+                    sum_near(g, cut).start()
+        else:
+            hold[:, at] = away
+
+    def pass_on(g, cut):
         at = pl.ds(cut * tile, tile)
         sum_near(g, cut).wait_recv()
-        total = keep[g, :, at] + recv1[g, :, at].astype(jnp.float32)
-
-        @pl.when(close[g])
-        def _():
-            keep[g, :, at] = total
-
-        @pl.when(jnp.logical_not(close[g]))
-        def _():
-            send2[:, at] = total.astype(jnp.bfloat16)
-            sum_far(cut).start()
+        send2[:, at] = (keep[g, :, at] + recv1[g, :, at].astype(jnp.float32)).astype(jnp.bfloat16)
+        sum_far(cut).start()
 
     def finish(cut):
         at = pl.ds(cut * tile, tile)
+        sum_near(kept, cut).wait_recv()
         sum_far(cut).wait_recv()
-        total = keep[(x + f // CORES) % PLANES, :, at] + recv2[:, at].astype(jnp.float32)
+        total = keep[kept, :, at] + recv1[kept, :, at].astype(jnp.float32) + recv2[:, at].astype(jnp.float32)
         out_ref[:, at] = total.astype(jnp.bfloat16)
 
+    def twin_in(cut):
+        landed = tile_at(0, height, other + (1 - k), cut)
+        pltpu.make_async_copy(landed, landed, twin_recv.at[cut]).wait()
+
+    def sent(ref, sem):
+        pltpu.make_async_copy(ref, ref, sem).wait()
+
+    def drain():
+        sent(up_src, cross_send)
+
+        @pl.when(t == f)
+        def _():
+            sent(up_src.at[0], home_send)
+
+        @pl.when(t != f)
+        def _():
+            sent(up_src, home_send)
+
+        @pl.when(jnp.logical_or(other == f, other + 1 == f))
+        def _():
+            sent(relayed.at[0], relay_send)
+
+        @pl.when(jnp.logical_and(other != f, other + 1 != f))
+        def _():
+            sent(relayed, relay_send)
+
+        for sem in (y_send, a_send, b_send):
+            sent(got_up.at[:, 0], sem)
+        sent(own_columns, own_send)
+        for sem in (split_send, dy_send, da_send, db_send):
+            sent(got_down.at[pl.ds(0, part), pl.ds(0, width)], sem)
+        for sem in (shared_send, ds_send):
+            sent(got_down.at[pl.ds(0, both), pl.ds(0, width)], sem)
+
     waiting, seen, ready, crossed, shared = [], [0] * up_cuts, [], [], []
+    tasks = [functools.partial(down_cast, step) for step in range(slabs)] + [functools.partial(normalize_rows, step) for step in range(NORMS)]
+    stages = STAGES if up_cuts % STAGES == 0 and height == up_cuts * cols else 1
+    span = up_cuts // stages
+
+    def finished(cut):
+        up_done(cut)
+        if (cut + 1) % span == 0 and cut + 1 < up_cuts:
+            if cut + 1 == span:
+                tasks.append(down_own.wait_recv)
+            for piece in range(down_cuts):
+                tasks.append(functools.partial(features, 0, piece, (cut + 1 - span) * cols, (cut + 1) * cols))
+
+    def spend(count):
+        for _ in range(min(count, len(tasks))):
+            tasks.pop(0)()
 
     def follow():
         kind, j, cut = waiting.pop(0)
@@ -353,7 +417,10 @@
 
             if cut + 1 < up_cuts:
                 up_direct(cut + 1)
+            spend(1)
         elif kind == "send":
+            if j == 0:
+                spend(len(tasks))
             for piece in range(down_cuts):
                 (down_split, down_shared)[j](piece).start()
         elif kind == "split":
@@ -370,76 +437,81 @@
             if len(waiting) > LAG:
                 follow()
             if len(ready) > 1:
-                up_done(ready.pop(0))
+                finished(ready.pop(0))
+            else:
+                spend(1)
 
     for cut in late:
         down_y(cut).start()
         waiting.append(("cross", 0, cut))
     while sum(seen) < fs * up_cuts:
         follow()
+        spend(2)
         while ready:
-            up_done(ready.pop(0))
-    down_own.wait_recv()
-
-    merging, merged, paired = [], [0] * down_cuts, 0
-
-    def settle(limit):
-        while len(merging) > limit:
-            g, cut = merging.pop(0)
-            merge(g, cut)
-            merged[cut] += 1
+            finished(ready.pop(0))
+    spend(len(tasks))
+    if stages == 1:
+        down_own.wait_recv()
+    for cut in range(down_cuts):
+        features(0, cut, height - height // stages, height)
+
+    def cross_in(step):
+        while step not in crossed:
+            follow()
 
     for step in range(down_cuts):
-        features(0, step)
-        merging.append((0, step))
-        if step % 2 == 1:
-            if waiting:
-                follow()
-            settle(3)
-    while paired < down_cuts:
-        if len(shared) < down_cuts and len(shared) <= len(crossed):
-            shared_in(len(shared))
-        if waiting:
-            follow()
-        if paired + 1 < len(crossed) or not waiting:
-            down_a(paired).wait_recv()
-            down_s(paired).wait_recv()
-            down_b(paired).wait_recv()
-            features(1, paired)
-            merging.append((1, paired))
-            paired += 1
-        settle(2)
-    settle(0)
-    for cut in range(down_cuts):
-        finish(cut)
-
-    for cut in range(up_cuts):
-        for lane in range(CORES):
-            up_cross(lane, cut).wait_send()
-
-            @pl.when(jnp.logical_or(t != f, lane != k))
+        if step not in shared:
+            shared_in(step)
+        cross_in(step)
+        @pl.when(jnp.logical_not(close))
+        def _():
+            pass_on(0, step)
+
+        if step >= DELAY:
+            @pl.when(close)
             def _():
-                up_home(lane, cut).wait_send()
-
-        for slot in range(CORES):
-            @pl.when(other + slot != f)
+                pass_on(1, step - DELAY)
+
+        twin_in(step)
+        features(1, step, 0, height)
+        if step + AHEAD < down_cuts:
+            @pl.when(close)
             def _():
-                up_relay(slot, cut).wait_send()
-        for j in range(fs):
-            up_y(rows_from[j], cut).wait_send()
-            up_a(rows_from[j], cut).wait_send()
-            up_b(rows_from[j], cut).wait_send()
-    down_own.wait_send()
-    for cut in range(down_cuts):
-        down_split(cut).wait_send()
-        down_shared(cut).wait_send()
-        down_y(cut).wait_send()
-        down_a(cut).wait_send()
-        down_s(cut).wait_send()
-        down_b(cut).wait_send()
-        sum_near(0, cut).wait_send()
-        sum_near(1, cut).wait_send()
-        sum_far(cut).wait_send()
+                sum_near(0, step + AHEAD).start()
+
+    @pl.when(close)
+    def _():
+        for step in range(down_cuts - DELAY, down_cuts):
+            pass_on(1, step)
+
+    drain()
+    for step in range(1, down_cuts):
+        finish(step - 1)
+    finish(down_cuts - 1)
+    sent(send1, send1_send)
+    sent(send2, send2_send)
+
+
+def put_out(src_ref, out_ref, sems):
+    chunks = sems.shape[0]
+    step = src_ref.shape[0] // chunks
+    for chunk in range(chunks):
+        at = pl.ds(chunk * step, step)
+        pltpu.make_async_copy(src_ref.at[at], out_ref.at[at], sems.at[chunk]).start()
+    for chunk in range(chunks):
+        at = pl.ds(chunk * step, step)
+        pltpu.make_async_copy(src_ref.at[at], out_ref.at[at], sems.at[chunk]).wait()
+
+
+def put(array):
+    return pl.pallas_call(
+        put_out,
+        out_shape=jax.ShapeDtypeStruct(array.shape, array.dtype),
+        in_specs=[pl.BlockSpec(memory_space=pltpu.VMEM)],
+        out_specs=pl.BlockSpec(memory_space=pltpu.HBM),
+        scratch_shapes=[pltpu.SemaphoreType.DMA((4,))],
+        compiler_params=pltpu.CompilerParams(vmem_limit_bytes=1 << 20),
+    )(array)
 
 
 def fused(tokens_in, up_master, down_master, norm_gain, dims):
@@ -452,9 +524,9 @@
     slabs = pieces_of(height, LINE, 8)
     dma = pltpu.SemaphoreType.DMA
     lanes, whole, strip = dma((CORES, up_cuts)), dma((fs, up_cuts)), dma((down_cuts,))
-    up_sems = [lanes, lanes, whole, lanes, lanes] + [whole] * 6
-    down_sems = [dma, dma] + [strip] * 12
-    sum_sems = [dma((2, down_cuts)), dma((2, down_cuts)), strip, strip]
+    up_sems = [dma] * 6 + [whole, lanes, whole, dma((up_cuts,))]
+    down_sems = [dma] * 8 + [strip] * 4
+    sum_sems = [dma, dma((2, down_cuts)), dma, strip]
     vmem = pl.BlockSpec(memory_space=pltpu.VMEM)
     hbm = pl.BlockSpec(memory_space=pl.ANY)
     got_up, got_down, out = pl.pallas_call(
@@ -474,6 +546,7 @@
             pltpu.VMEM((CORES, rows, cols), jnp.bfloat16),
             pltpu.VMEM((2, height // slabs, width), jnp.float32),
             pltpu.VMEM((tokens, cols), jnp.bfloat16),
+            pltpu.VMEM((tokens, width), jnp.float32),
             pltpu.VMEM((2, tokens, width), jnp.float32),
             pltpu.VMEM((2, tokens, width), jnp.bfloat16),
             pltpu.VMEM((2, tokens, width), jnp.bfloat16),
@@ -482,11 +555,11 @@
             up_sems,
             down_sems,
             sum_sems,
-            [lanes, dma((2,)), dma],
+            [dma((up_cuts,)), dma((2,)), dma],
         ],
         compiler_params=pltpu.CompilerParams(collective_id=0, has_side_effects=True, vmem_limit_bytes=LIMIT << 20),
     )(tokens_in, norm_gain, up_master.reshape(groups * CORES, rows, cols), down_master)
-    return out, got_up.reshape(fs * groups * CORES * rows, cols), got_down
+    return out, put(got_up).reshape(fs * groups * CORES * rows, cols), put(got_down)
 
 
 def fits(up_shape, down_shape, dims):

time: 179 us -> 172 us (0.961)
  the two profiles are of different devices: /device:TPU:3 before, /device:TPU:0 now
where the time goes in v3:
time: 172 us
  Pallas kernels  170 us (99%)
    pallas_call x1, Pallas kernels, fused(): pl.pallas_call(functools.partial(hand_over, dims, (up_cuts, down_cuts)),...  157 us
    pallas_call x2, Pallas kernels, put(): pl.pallas_call(put_out, out_shape=jax.ShapeDtypeStruct(array.shape, array...  13.2 us

profile of v3, /device:TPU:0, one launch (start us, length us, event | category | flops | bytes accessed | tf_op | source)
XLA Modules:
  0.0 171.6 jit_solution(9303408905611375818)
XLA Ops:
  0.6 156.9 %shard_map.67 = (bf16[4,4,192,3072]{3,2,1,0:T(8,128)(2,1)S(1)}, bf16[3072,3072]{1,0:T(8,128)(2,1)S(1)}, bf16[256,768]{1,0:T(8,128)(2,1)}) custom-call(bf16[256,3072]{1,0:T(8,128)(2,1)} %tokens_ref.1, f32[768]{0:T(1024)} %gain_ref.1, f32[4,192,3072]{2,1,0:T(8,128)} %bitcast.3, f32[3072,768]{1,0:T(8,128)} %master_ref.1), custom_call_target="tpu_custom_call" | custom-call | tf_op jit(solution)/shard_map/pallas_call | solution.py:532
  157.6 6.6 %shard_map.68 = bf16[4,4,192,3072]{3,2,1,0:T(8,128)(2,1)} custom-call(bf16[4,4,192,3072]{3,2,1,0:T(8,128)(2,1)S(1)} %get-tuple-element.7.src_ref), custom_call_target="tpu_custom_call" | custom-call | tf_op jit(solution)/shard_map/pallas_call | solution.py:507
  164.2 0.0 copy-start
  164.2 6.6 %shard_map.69 = bf16[3072,3072]{1,0:T(8,128)(2,1)} custom-call(bf16[3072,3072]{1,0:T(8,128)(2,1)S(1)} %get-tuple-element.8.src_ref), custom_call_target="tpu_custom_call" | custom-call | tf_op jit(solution)/shard_map/pallas_call | solution.py:507
  170.8 0.0 copy-done
  170.9 0.7 copy.8
Async XLA Ops:
  164.2 6.6 %copy-start = (bf16[256,768]{1,0:T(8,128)(2,1)S(1)}, bf16[256,768]{1,0:T(8,128)(2,1)}, u32[]{:S(2)}) copy-start(bf16[256,768]{1,0:T(8,128)(2,1)} %get-tuple-element.12) | copy-start | bytes 1179652

commit v4 on v3

--- a/solution.py
+++ b/solution.py
@@ -17,6 +17,8 @@
 STAGES = 4
 DELAY = 3
 AHEAD = 2
+LATE = 2
+FLOPS = 10_000_000_000
 NORMS = 4
 START = 0.12
 UP_CUTS = 12
@@ -71,7 +73,7 @@
     return order[:last], spare
 
 
-def hand_over(dims, cuts, tokens_ref, gain_ref, up_ref, master_ref, got_up, got_down, out_ref, rows_ref, gains, up_stage, up_src, relayed, stage, hidden, hold, keep, send1, recv1, send2, recv2, up_sems, down_sems, sum_sems, load_sems):
+def hand_over(dims, cuts, tokens_ref, gain_ref, up_ref, master_ref, got_up, got_down, out_ref, base_ref, late_ref, away_ref, rows_ref, gains, up_stage, up_src, relayed, stage, hidden, hold, keep, send1, recv1, send2, recv2, up_sems, down_sems, sum_sems, load_sems):
     groups, fs, tp = dims
     up_cuts, down_cuts = cuts
     y, f, t = lax.axis_index("grp"), lax.axis_index("fs"), lax.axis_index("tp")
@@ -296,6 +298,7 @@
         return remote(send2.at[:, at], recv2.at[:, at], send2_send, send2_recv.at[cut], (y, facing, t))
 
     bases = (x * CORES, other)
+    soon = down_cuts - LATE
     close = x == f // CORES
     kept = (x + f // CORES) % PLANES
 
@@ -311,6 +314,11 @@
     def features(g, cut, first, last):
         at = pl.ds(cut * tile, tile)
         away, here = terms(g, cut, first, last)
+        if g == 1 and cut >= soon:
+            place = pl.ds((cut - soon) * tile, tile)
+            late_ref[:, place] = here
+            away_ref[:, place] = away.astype(jnp.bfloat16)
+            return
         if first > 0:
             away, here = hold[:, at] + away, keep[g, :, at] + here
         keep[g, :, at] = here
@@ -336,7 +344,10 @@
         sum_near(kept, cut).wait_recv()
         sum_far(cut).wait_recv()
         total = keep[kept, :, at] + recv1[kept, :, at].astype(jnp.float32) + recv2[:, at].astype(jnp.float32)
-        out_ref[:, at] = total.astype(jnp.bfloat16)
+        if cut < soon:
+            out_ref[:, at] = total.astype(jnp.bfloat16)
+        else:
+            base_ref[:, pl.ds((cut - soon) * tile, tile)] = total
 
     def twin_in(cut):
         landed = tile_at(0, height, other + (1 - k), cut)
@@ -467,7 +478,7 @@
         def _():
             pass_on(0, step)
 
-        if step >= DELAY:
+        if DELAY <= step < DELAY + soon:
             @pl.when(close)
             def _():
                 pass_on(1, step - DELAY)
@@ -481,15 +492,26 @@
 
     @pl.when(close)
     def _():
-        for step in range(down_cuts - DELAY, down_cuts):
+        for step in range(max(down_cuts - DELAY, 0), soon):
             pass_on(1, step)
 
     drain()
-    for step in range(1, down_cuts):
-        finish(step - 1)
-    finish(down_cuts - 1)
-    sent(send1, send1_send)
-    sent(send2, send2_send)
+    for step in range(soon):
+        finish(step)
+
+    sent(rows_ref.at[:, pl.ds(0, (down_cuts + soon) * tile)], send1_send)
+
+    @pl.when(close)
+    def _():
+        for step in range(soon, down_cuts):
+            finish(step)
+        if soon:
+            sent(send2.at[:, pl.ds(0, soon * tile)], send2_send)
+
+    @pl.when(jnp.logical_not(close))
+    def _():
+        base_ref[...] = jnp.zeros_like(base_ref)
+        sent(send2, send2_send)
 
 
 def put_out(src_ref, out_ref, sems):
@@ -511,6 +533,7 @@
         out_specs=pl.BlockSpec(memory_space=pltpu.HBM),
         scratch_shapes=[pltpu.SemaphoreType.DMA((4,))],
         compiler_params=pltpu.CompilerParams(vmem_limit_bytes=1 << 20),
+        cost_estimate=pl.CostEstimate(flops=FLOPS, bytes_accessed=2 * array.size, transcendentals=0),
     )(array)
 
 
@@ -529,15 +552,19 @@
     sum_sems = [dma, dma((2, down_cuts)), dma, strip]
     vmem = pl.BlockSpec(memory_space=pltpu.VMEM)
     hbm = pl.BlockSpec(memory_space=pl.ANY)
-    got_up, got_down, out = pl.pallas_call(
+    late = width // down_cuts * LATE
+    got_up, got_down, out, base, rest, away = pl.pallas_call(
         functools.partial(hand_over, dims, (up_cuts, down_cuts)),
         out_shape=(
             pltpu.VMEM((fs, groups * CORES, rows, cols), jnp.bfloat16),
             pltpu.VMEM((height, tp * width), jnp.bfloat16),
-            jax.ShapeDtypeStruct((tokens, width), jnp.bfloat16),
+            pltpu.VMEM((tokens, width - late), jnp.bfloat16),
+            pltpu.VMEM((tokens, late), jnp.float32),
+            pltpu.VMEM((tokens, late), jnp.float32),
+            pltpu.VMEM((tokens, late), jnp.bfloat16),
         ),
         in_specs=[hbm, vmem, hbm, hbm],
-        out_specs=(vmem, vmem, vmem),
+        out_specs=(vmem,) * 6,
         scratch_shapes=[
             pltpu.VMEM(tokens_in.shape, jnp.bfloat16),
             pltpu.VMEM((up_master.shape[0], 128), jnp.float32),
@@ -559,7 +586,14 @@
         ],
         compiler_params=pltpu.CompilerParams(collective_id=0, has_side_effects=True, vmem_limit_bytes=LIMIT << 20),
     )(tokens_in, norm_gain, up_master.reshape(groups * CORES, rows, cols), down_master)
-    return out, put(got_up).reshape(fs * groups * CORES * rows, cols), put(got_down)
+    near = lax.ppermute(away, "fs", [(i, i + 1 - 2 * (i % 2)) for i in range(fs)])
+    up = put(got_up).reshape(fs * groups * CORES * rows, cols)
+    merged = rest + near.astype(jnp.float32)
+    far = lax.ppermute(merged.astype(jnp.bfloat16), "fs", [(i, (i + 2) % fs) for i in range(fs)])
+    down = put(got_down)
+    home = lax.axis_index("tp") // CORES == lax.axis_index("fs") // CORES
+    tail = jnp.where(home, base, merged + far.astype(jnp.float32)).astype(jnp.bfloat16)
+    return jnp.concatenate([out, tail], axis=1), up, down
 
 
 def fits(up_shape, down_shape, dims):
@@ -567,7 +601,7 @@
     own = 2 * (up_shape[0] * up_shape[1] * fs + down_shape[0] * down_shape[1] * tp)
     aligned = up_shape[0] % (groups * CORES * LINE) == 0 and up_shape[0] % 128 == 0 and up_shape[1] % UNIT == 0
     square = groups == 2 and tp == CORES * PLANES and fs == tp
-    return square and aligned and down_shape[0] % UNIT == 0 and down_shape[1] % 128 == 0 and own <= 40 << 20
+    return square and aligned and down_shape[0] % UNIT == 0 and down_shape[1] % 128 == 0 and own <= 40 << 20 and pieces_of(down_shape[1], 128, DOWN_CUTS) == DOWN_CUTS
 
 
 def by_collectives(normalized, up_cast, down_cast):

time: 172 us -> 171 us (level)
  the two profiles are of different devices: /device:TPU:0 before, /device:TPU:3 now
where the time goes in v4:
time: 171 us; the launch traced here: 168 us
  Pallas kernels  162 us (95%)
  starting transfers between devices  3.26 us (2%)
    pallas_call x1, Pallas kernels, fused(): pl.pallas_call(functools.partial(hand_over, dims, (up_cuts, down_cuts)),...  148 us
    pallas_call x2, Pallas kernels, put(): pl.pallas_call(put_out, out_shape=jax.ShapeDtypeStruct(array.shape, array...  13.2 us
  transfers between devices with their start and end apart: 2, of which 1 were waited for; matrix products, arithmetic and copies ran while one was open for 0% of the time, Pallas kernels for 8%

profile of v4, /device:TPU:3, one launch (start us, length us, event | category | flops | bytes accessed | tf_op | source)
XLA Modules:
  0.0 167.8 jit_solution(2061002175771855849)
XLA Ops:
  0.6 148.4 %shard_map.67 = (bf16[4,4,192,3072]{3,2,1,0:T(8,128)(2,1)S(1)}, bf16[3072,3072]{1,0:T(8,128)(2,1)S(1)}, bf16[256,512]{1,0:T(8,128)(2,1)S(1)}, f32[256,256]{1,0:T...) custom-call(bf16[256,3072]{1,0:T(8,128)(2,1)} %tokens_ref.1, f32[768]{0:T(1024)} %gain_ref.1, ...), custom_call_target="tpu_custom_call" | custom-call | tf_op jit(solution)/shard_map/pallas_call | solution.py:556
  149.0 3.2 %collective-permute-start = (bf16[256,256]{1,0:T(8,128)(2,1)S(1)}, bf16[256,256]{1,0:T(8,128)(2,1)S(1)}, u32[]{:S(2)}, u32[]{:S(2)}) collective-permute-start(bf16[256,256]{1,0:T(8,128)(2,1)S(1)} %get-tuple-element.12), channel_id=1, source_target_pairs={{0,4},{4,0},{8,12},{12,8},{1,5},{5,1},{9,13},{13,9},{2,6},{6,2},{1... | collective-permute-start | bytes 393224 | tf_op jit(solution)/shard_map/ppermute | solution.py:589
  152.2 6.6 %shard_map.68 = bf16[4,4,192,3072]{3,2,1,0:T(8,128)(2,1)} custom-call(bf16[4,4,192,3072]{3,2,1,0:T(8,128)(2,1)S(1)} %get-tuple-element.13.src_ref), custom_call_target="tpu_custom_call" | custom-call | flops 10000000000 | bytes 18874368 | tf_op jit(solution)/shard_map/pallas_call | solution.py:529
  158.8 0.0 collective-permute-done
  158.9 0.1 collective-permute-start.1
  158.9 6.6 %shard_map.69 = bf16[3072,3072]{1,0:T(8,128)(2,1)} custom-call(bf16[3072,3072]{1,0:T(8,128)(2,1)S(1)} %get-tuple-element.14.src_ref), custom_call_target="tpu_custom_call" | custom-call | flops 10000000000 | bytes 18874368 | tf_op jit(solution)/shard_map/pallas_call | solution.py:529
  165.6 1.3 collective-permute-done.1
  166.9 0.1 select_convert_fusion
  167.0 0.8 pad_maximum_fusion
  (1 shorter events, 0.0 us)
Async XLA Ops:
  149.0 9.8 %collective-permute-start = (bf16[256,256]{1,0:T(8,128)(2,1)S(1)}, bf16[256,256]{1,0:T(8,128)(2,1)S(1)}, u32[]{:S(2)}, u32[]{:S(2)}) collective-permute-start(bf16[256,256]{1,0:T(8,128)(2,1)S(1)} %get-tuple-element.12), channel_id=1, source_target_pairs={{0,4},{4,0},{8,12},{12,8},{1,5},{5,1},{9,13},{13,9},{2,6},{6,2},{1... | collective-permute-start | bytes 393224 | tf_op jit(solution)/shard_map/ppermute | solution.py:589
  158.9 8.1 %collective-permute-start.1 = (bf16[256,256]{1,0:T(8,128)(2,1)S(1)}, bf16[256,256]{1,0:T(8,128)(2,1)S(1)}, u32[]{:S(2)}, u32[]{:S(2)}) collective-permute-start(bf16[256,256]{1,0:T(8,128)(2,1)S(1)} %fusion), channel_id=1, source_target_pairs={{0,8},{4,12},{8,0},{12,4},{1,9},{5,13},{9,1},{13,5},{2,10},{6,14},... | collective-permute-start | bytes 393224 | tf_op jit(solution)/shard_map/ppermute | solution.py:592

commit v5 on v4

--- a/solution.py
+++ b/solution.py
@@ -18,6 +18,7 @@
 DELAY = 3
 AHEAD = 2
 LATE = 2
+EAGER = 2
 FLOPS = 10_000_000_000
 NORMS = 4
 START = 0.12
@@ -233,10 +234,12 @@
         def _():
             up_local(cut).start()
 
-    for cut in range(up_cuts):
+    for cut in range(min(EAGER, up_cuts)):
         up_cast(cut)
     pl.semaphore_wait(barrier, len(partners))
     for cut in range(up_cuts):
+        if cut >= EAGER:
+            up_cast(cut)
         up_start(cut)
         if cut == 0:
             up_direct(cut)

time: 171 us -> 170 us (level)
  Pallas kernels: 162 us -> 160 us
where the time goes in v5:
time: 170 us; the launch traced here: 167 us
  Pallas kernels  160 us (94%)
  starting transfers between devices  3.87 us (2%)
    pallas_call x1, Pallas kernels, fused(): pl.pallas_call(functools.partial(hand_over, dims, (up_cuts, down_cuts)),...  147 us
    pallas_call x2, Pallas kernels, put(): pl.pallas_call(put_out, out_shape=jax.ShapeDtypeStruct(array.shape, array...  13.2 us
    ppermute x1, starting transfers between devices, fused(): lax.ppermute(away, 'fs', [(i, i + 1 - 2 * (i % 2)) for i in range(fs)])  3.8 us
  transfers between devices with their start and end apart: 2, of which 1 were waited for; matrix products, arithmetic and copies ran while one was open for 0% of the time, Pallas kernels for 8%

profile of v5, /device:TPU:3, one launch (start us, length us, event | category | flops | bytes accessed | tf_op | source)
XLA Modules:
  0.0 166.8 jit_solution(16950717938928237951)
XLA Ops:
  0.6 147.0 %shard_map.67 = (bf16[4,4,192,3072]{3,2,1,0:T(8,128)(2,1)S(1)}, bf16[3072,3072]{1,0:T(8,128)(2,1)S(1)}, bf16[256,512]{1,0:T(8,128)(2,1)S(1)}, f32[256,256]{1,0:T...) custom-call(bf16[256,3072]{1,0:T(8,128)(2,1)} %tokens_ref.1, f32[768]{0:T(1024)} %gain_ref.1, ...), custom_call_target="tpu_custom_call" | custom-call | tf_op jit(solution)/shard_map/pallas_call | solution.py:559
  147.7 3.8 %collective-permute-start = (bf16[256,256]{1,0:T(8,128)(2,1)S(1)}, bf16[256,256]{1,0:T(8,128)(2,1)S(1)}, u32[]{:S(2)}, u32[]{:S(2)}) collective-permute-start(bf16[256,256]{1,0:T(8,128)(2,1)S(1)} %get-tuple-element.12), channel_id=1, source_target_pairs={{0,4},{4,0},{8,12},{12,8},{1,5},{5,1},{9,13},{13,9},{2,6},{6,2},{1... | collective-permute-start | bytes 393224 | tf_op jit(solution)/shard_map/ppermute | solution.py:592
  151.5 6.6 %shard_map.68 = bf16[4,4,192,3072]{3,2,1,0:T(8,128)(2,1)} custom-call(bf16[4,4,192,3072]{3,2,1,0:T(8,128)(2,1)S(1)} %get-tuple-element.13.src_ref), custom_call_target="tpu_custom_call" | custom-call | flops 10000000000 | bytes 18874368 | tf_op jit(solution)/shard_map/pallas_call | solution.py:532
  158.1 0.0 collective-permute-done
  158.1 0.1 collective-permute-start.1
  158.2 6.6 %shard_map.69 = bf16[3072,3072]{1,0:T(8,128)(2,1)} custom-call(bf16[3072,3072]{1,0:T(8,128)(2,1)S(1)} %get-tuple-element.14.src_ref), custom_call_target="tpu_custom_call" | custom-call | flops 10000000000 | bytes 18874368 | tf_op jit(solution)/shard_map/pallas_call | solution.py:532
  164.8 1.2 collective-permute-done.1
  166.0 0.1 select_convert_fusion
  166.1 0.8 pad_maximum_fusion
  (1 shorter events, 0.0 us)
Async XLA Ops:
  147.7 10.4 %collective-permute-start = (bf16[256,256]{1,0:T(8,128)(2,1)S(1)}, bf16[256,256]{1,0:T(8,128)(2,1)S(1)}, u32[]{:S(2)}, u32[]{:S(2)}) collective-permute-start(bf16[256,256]{1,0:T(8,128)(2,1)S(1)} %get-tuple-element.12), channel_id=1, source_target_pairs={{0,4},{4,0},{8,12},{12,8},{1,5},{5,1},{9,13},{13,9},{2,6},{6,2},{1... | collective-permute-start | bytes 393224 | tf_op jit(solution)/shard_map/ppermute | solution.py:592
  158.1 7.9 %collective-permute-start.1 = (bf16[256,256]{1,0:T(8,128)(2,1)S(1)}, bf16[256,256]{1,0:T(8,128)(2,1)S(1)}, u32[]{:S(2)}, u32[]{:S(2)}) collective-permute-start(bf16[256,256]{1,0:T(8,128)(2,1)S(1)} %fusion), channel_id=1, source_target_pairs={{0,8},{4,12},{8,0},{12,4},{1,9},{5,13},{9,1},{13,5},{2,10},{6,14},... | collective-permute-start | bytes 393224 | tf_op jit(solution)/shard_map/ppermute | solution.py:595
